TPU v7x, 32 devices: a whole 2x2x4 slice. The times are simulated.
32 devices in a mesh: sp: 16 (over z, y, x), tp: 2 (over core).
Axes of the slice: x: 2, y: 2, z: 4, core: 2. Of those that a mesh axis runs over, the one named last changes fastest.
Arguments:
- residual: bfloat16 [4096, 2048], P(('sp', 'tp')), may hold values from -6 to 6
- queries: bfloat16 [4096, 1152], P('sp', 'tp'), may hold values from -800 to 800
- latent: bfloat16 [4096, 256], P('sp'), may hold values from -6 to 6
- rope_key: bfloat16 [4096, 32], P('sp'), may hold values from -6 to 6
- doc_ids: int32 [4096], P('sp'), may hold values from 0 to 5, never falling along the last dimension, each value on 1 to 2048 neighbouring positions
- latent_to_key: bfloat16 [256, 768], P(None, 'tp'), may hold values from -0.375 to 0.375
- latent_to_value: bfloat16 [256, 768], P(None, 'tp'), may hold values from -0.375 to 0.375
- out_proj: bfloat16 [768, 2048], replicated, may hold values from -0.21875 to 0.21875
- mix_gain: float32 [2048], replicated, may hold values from 0.1 to 1.9
- moe_gain: float32 [2048], replicated, may hold values from 0.1 to 1.9
- expert_ids: int32 [4096, 2], P(('sp', 'tp')), may hold values from 0 to 15, as said below
- route_weight: float32 [4096, 2], P(('sp', 'tp')), may hold values from 0.1 to 1
- gate_weight: bfloat16 [16, 2048, 1024], P('sp', None, 'tp'), may hold values from -0.125 to 0.125
- up_weight: bfloat16 [16, 2048, 1024], P('sp', None, 'tp'), may hold values from -0.125 to 0.125
- down_weight: bfloat16 [16, 1024, 2048], P('sp', 'tp'), may hold values from -0.1875 to 0.1875
Outputs:
- output: bfloat16 [4096, 2048], P(('sp', 'tp'))
Inputs may be any that keep to these rules, and one draw needn't show every extreme that they name: `expert_ids`: each row names 2 different experts of one group of 4 consecutive numbers; in each aligned block of 128 rows (the rows of one device) no expert is named more than 32 times, and some expert exactly 32 times.
All inputs are finite; a program needn't handle non-finite values.
Results may differ from a plain program's by a relative error of at most 0.013.
Values may be sent and summed in bfloat16 or wider, within the bound.
A program may use at most 64 MiB of HBM per device.

v0:
```python
import math

import jax
import jax.numpy as jnp
from jax import lax
from jax.sharding import PartitionSpec as P

D = 2048
UNROTATED_DIM = 64
ROPE = 32
VALUE_ENTRIES = 64
GROUPS = 4


rope_base = 10000.0
epsilon = 1e-06


def rotate(source, positions):
    half_width = source.shape[-1] // 2
    frequency = rope_base ** (-jnp.arange(half_width, dtype=jnp.float32) / half_width)
    angles = positions.astype(jnp.float32)[:, None] * frequency[None, :]
    if source.ndim == 3:
        angles = angles[:, None, :]
    cosine = jnp.cos(angles)
    sine_part = jnp.sin(angles)
    upper_half = source[..., :half_width].astype(jnp.float32)
    lower_half = source[..., half_width:].astype(jnp.float32)
    turned = jnp.concatenate(
        [
            upper_half * cosine - lower_half * sine_part,
            lower_half * cosine + upper_half * sine_part,
        ],
        axis=-1,
    )
    return turned.astype(jnp.bfloat16)


def rms_scale(source, gain):
    return source * lax.rsqrt(jnp.mean(source * source, axis=-1, keepdims=True) + epsilon) * gain


def attend_keys(
    running,
    query_nope,
    query_rot,
    query_pos,
    query_docs,
    key_nope,
    key_rot,
    value_rows,
    key_pos,
    key_docs,
):
    row_max, row_total, weighted = running
    score_scale = (UNROTATED_DIM + ROPE) ** (-0.5)
    scores = (
        jnp.einsum("qhd,khd->qhk", query_nope, key_nope, preferred_element_type=jnp.float32)
        + jnp.einsum("qhr,kr->qhk", query_rot, key_rot, preferred_element_type=jnp.float32)
    ) * score_scale
    allowed = (
        (key_pos[None, :] <= query_pos[:, None]) & (key_docs[None, :] == query_docs[:, None])
    )[:, None, :]
    new_max = jnp.maximum(row_max, jnp.max(jnp.where(allowed, scores, -1e30), axis=-1))
    weights = jnp.where(allowed, jnp.exp(scores - new_max[..., None]), 0.0)
    factor = jnp.exp(row_max - new_max)
    row_total = row_total * factor + jnp.sum(weights, axis=-1)
    weighted = weighted * factor[..., None] + jnp.einsum(
        "qhk,khd->qhd", weights.astype(jnp.bfloat16), value_rows, preferred_element_type=jnp.float32
    )
    return (new_max, row_total, weighted)


def local(
    residual,
    queries,
    latent,
    rope_key,
    doc_ids,
    latent_to_key,
    latent_to_value,
    out_proj,
    mix_gain,
    moe_gain,
    expert_ids,
    route_weight,
    gate_weight,
    up_weight,
    down_weight,
):
    local_rows = queries.shape[0]
    local_heads = queries.shape[1] // (UNROTATED_DIM + ROPE)
    query_pos = lax.axis_index("sp") * local_rows + jnp.arange(local_rows, dtype=jnp.int32)
    shaped = queries.reshape(local_rows, local_heads, UNROTATED_DIM + ROPE)
    query_nope = shaped[..., :UNROTATED_DIM]
    query_rot = rotate(shaped[..., UNROTATED_DIM:], query_pos)
    key_rot = rotate(rope_key, query_pos)
    initial = (
        jnp.full((local_rows, local_heads), -1e30, jnp.float32),
        jnp.zeros((local_rows, local_heads), jnp.float32),
        jnp.zeros((local_rows, local_heads, VALUE_ENTRIES), jnp.float32),
    )
    pieces = (
        lax.all_gather(latent, "sp", axis=0, tiled=True),
        lax.all_gather(key_rot, "sp", axis=0, tiled=True),
        lax.all_gather(doc_ids, "sp", axis=0, tiled=True),
    )
    row_count = pieces[0].shape[0]
    block_rows = math.gcd(row_count, 512)

    def one_block(number, current):
        first_row = number * block_rows
        sliced = [lax.dynamic_slice_in_dim(member, first_row, block_rows, 0) for member in pieces]
        key_pos = first_row + jnp.arange(block_rows, dtype=jnp.int32)
        active = (first_row <= query_pos[-1]) & (sliced[-1][-1] >= doc_ids[0])

        def compute(carried):
            key_nope = jnp.dot(sliced[0], latent_to_key, preferred_element_type=jnp.float32).astype(
                jnp.bfloat16
            )
            value_rows = jnp.dot(
                sliced[0], latent_to_value, preferred_element_type=jnp.float32
            ).astype(jnp.bfloat16)
            key_part = sliced[1]
            return attend_keys(
                carried,
                query_nope,
                query_rot,
                query_pos,
                doc_ids,
                key_nope.reshape(block_rows, local_heads, UNROTATED_DIM),
                key_part,
                value_rows.reshape(block_rows, local_heads, VALUE_ENTRIES),
                key_pos,
                sliced[-1],
            )

        return lax.cond(active, compute, lambda carried: carried, current)

    running = lax.fori_loop(0, row_count // block_rows, one_block, initial)
    attended = (running[2] / running[1][..., None]).astype(jnp.bfloat16)
    attended = attended.reshape(local_rows, local_heads * VALUE_ENTRIES)
    gathered = lax.all_to_all(attended, "tp", split_axis=0, concat_axis=1, tiled=True)
    mix = jnp.dot(gathered, out_proj, preferred_element_type=jnp.float32)
    branch = rms_scale(mix, mix_gain)
    middle = lax.optimization_barrier((residual.astype(jnp.float32) + branch).astype(jnp.bfloat16))
    normed = rms_scale(middle.astype(jnp.float32), moe_gain).astype(jnp.bfloat16)
    row_count = normed.shape[0]
    top_count = expert_ids.shape[1]
    expert_count = lax.axis_size("sp")
    capacity = row_count // (expert_count // GROUPS)
    flat_ids = expert_ids.reshape(-1)
    onehot = (flat_ids[:, None] == jnp.arange(expert_count, dtype=jnp.int32)[None, :]).astype(
        jnp.int32
    )
    earlier = jnp.cumsum(onehot, axis=0) - onehot
    slot_rank = jnp.sum(earlier * onehot, axis=1)
    slot_ids = (flat_ids * capacity + slot_rank).reshape(row_count, top_count)
    chooser = jnp.any(
        jnp.arange(expert_count * capacity, dtype=jnp.int32)[:, None, None] == slot_ids[None],
        axis=2,
    ).astype(jnp.bfloat16)
    buffer = jnp.dot(chooser, normed, preferred_element_type=jnp.float32).astype(jnp.bfloat16)
    buffer = buffer.reshape(expert_count, capacity, D)
    arrived = lax.all_to_all(buffer, "sp", split_axis=0, concat_axis=0, tiled=True)
    model_width = arrived.shape[2]
    both_halves = lax.all_gather(arrived, "tp", axis=0, tiled=True)
    flat_rows = both_halves.reshape(-1, model_width)
    gate_out = jnp.dot(flat_rows, gate_weight[0], preferred_element_type=jnp.float32)
    upward = jnp.dot(flat_rows, up_weight[0], preferred_element_type=jnp.float32)
    hidden = (jax.nn.silu(gate_out) * upward).astype(jnp.bfloat16)
    partial_value = jnp.dot(hidden, down_weight[0], preferred_element_type=jnp.float32).reshape(
        both_halves.shape
    )
    summed = lax.psum_scatter(
        partial_value.astype(jnp.bfloat16), "tp", scatter_dimension=0, tiled=True
    )
    returned = lax.all_to_all(summed, "sp", split_axis=0, concat_axis=0, tiled=True)
    picked = returned.reshape(-1, D)[slot_ids.reshape(-1)].astype(jnp.float32)
    expert_mix = jnp.sum(
        (picked * route_weight.reshape(-1)[:, None]).reshape(row_count, top_count, D), axis=1
    )
    return (middle.astype(jnp.float32) + expert_mix).astype(jnp.bfloat16)


def solution(mesh):
    in_specs = (
        P(("sp", "tp"), None),
        P("sp", "tp"),
        P("sp", None),
        P("sp", None),
        P("sp"),
        P(None, "tp"),
        P(None, "tp"),
        P(),
        P(),
        P(),
        P(("sp", "tp"), None),
        P(("sp", "tp"), None),
        P("sp", None, "tp"),
        P("sp", None, "tp"),
        P("sp", "tp", None),
    )
    out_specs = P(("sp", "tp"), None)
    return jax.shard_map(local, mesh=mesh, in_specs=in_specs, out_specs=out_specs, check_vma=False)
```

profile of v0, /device:TPU:0, one launch (start us, length us, event | category | flops | bytes accessed | tf_op | source)
XLA Modules:
  0.0 351.3 jit_solution(15454426010677830794)
XLA Ops:
  6.5 0.7 all-gather.4.cloned.1.call-update
  7.3 1.0 copy.41
  8.6 1.6 slice.54
  11.8 0.6 broadcast_multiply_fusion
  12.5 44.9 %all-gather = s32[16,1,256]{2,1,0:T(1,128)} all-gather(s32[1,1,256]{2,1,0:T(1,128)} %bitcast.85), channel_id=1, replica_groups=mesh['sp'=16,'tp'=2] {'sp'}, dimensions={0}, use_global_device_ids=true | all-gather | bytes 17408 | tf_op jit(solution)/shard_map/all_gather | solution.py:106
  58.0 0.9 multiply_cosine_fusion
  58.9 0.9 fusion.39
  59.8 0.7 pad_maximum_fusion
  60.4 0.7 fusion.37
  61.1 39.4 %all_gather.14 = bf16[4096,32]{0,1:T(8,128)(2,1)} all-gather(bf16[256,32]{0,1:T(8,128)(2,1)S(1)} %pad_maximum_fusion.1), channel_id=1, replica_groups=mesh['sp'=16,'tp'=2] {'sp'}, dimensions={0}, use_global_device_ids=true | all-gather | bytes 278528 | tf_op jit(solution)/shard_map/all_gather | solution.py:105
  100.6 57.7 %while.17 = (s32[]{:T(128)}, f32[256,6]{0,1:T(8,128)S(1)}, f32[256,6]{0,1:T(8,128)S(1)}, f32[256,6,64]{0,2,1:T(8,128)S(1)}, s32[256]{0:T(256)}, /*index=5*/s32[4...) while((s32[]{:T(128)}, f32[256,6]{0,1:T(8,128)S(1)}, ...), condition=%wide.region_5.6_spmd, body=%wide.region_0.5_spmd.sunk | while | flops 461835776 | bytes 21579896 | solution.py:140
  100.6 0.8 dynamic_slice.40
  101.9 0.6 slice.71
  102.6 1.2 slice.72
  104.9 1.3 slice.70
  106.9 7.0 %conditional.2 = ((f32[256,6]{0,1:T(8,128)S(1)}, f32[256,6]{0,1:T(8,128)S(1)}, f32[256,6,64]{0,2,1:T(8,128)S(1)})) conditional(s32[]{:T(128)} %convert_element_type.171, (f32[256,6]{0,1:T(8,128)S(1)}, f32[256,6]{0,1:T(8,128)S(1)}, f32[256,6,64]{0,2,1:T(8,128)S(1)}) %tuple.50, (s32[]{:T(128)}, s32[512]{0:T(512)}, s32[256]{0:T(256)}, s32[512]{0:T(512)}, ...), branch_computations={%region_1.0_spmd, %region_2.4_spmd} | conditional | flops 461835776 | bytes 21565132 | solution.py:138
  106.9 1.3 convolution_convert_fusion.1
  108.3 1.5 fusion.16
  110.1 0.9 select_reduce_fusion
  111.9 1.2 convolution_convert_fusion
  113.1 0.7 fusion.11
  113.9 0.8 dynamic_slice.40
  115.3 0.6 slice.71
  115.9 1.2 slice.72
  118.3 1.3 slice.70
  120.2 0.8 dynamic_slice.40
  121.6 0.6 slice.71
  122.2 1.2 slice.72
  124.6 1.3 slice.70
  126.6 0.8 dynamic_slice.40
  127.9 0.6 slice.71
  128.6 1.2 slice.72
  130.9 1.3 slice.70
  132.9 0.8 dynamic_slice.40
  134.3 0.6 slice.71
  134.9 1.2 slice.72
  137.3 1.3 slice.70
  139.2 0.8 dynamic_slice.40
  140.6 0.6 slice.71
  141.2 1.2 slice.72
  143.6 1.3 slice.70
  145.6 0.8 dynamic_slice.40
  147.6 1.2 slice.72
  149.9 1.3 slice.70
  151.9 0.8 dynamic_slice.40
  153.9 1.2 slice.72
  156.3 1.3 slice.70
  158.2 0.7 divide_convert_fusion
  158.9 1.0 all_to_all.20
  160.0 3.9 %all_to_all.29 = bf16[2,128,384]{1,2,0:T(8,128)(2,1)S(1)} all-to-all(bf16[2,128,384]{1,2,0:T(8,128)(2,1)S(1)} %copy.40), channel_id=1, replica_groups=mesh['sp'=16,'tp'=2] {'tp'}, dimensions={0} | all-to-all | bytes 393216 | tf_op jit(solution)/shard_map/all_to_all | solution.py:143
  163.9 0.7 multiply_reduce_fusion.1
  165.9 0.8 convolution_convert_fusion.3
  166.7 75.4 %all_to_all.30 = bf16[16,32,2048]{2,1,0:T(8,128)(2,1)} all-to-all(bf16[16,32,2048]{2,1,0:T(8,128)(2,1)S(1)} %bitcast.80), channel_id=1, replica_groups=mesh['sp'=16,'tp'=2] {'sp'}, dimensions={0} | all-to-all | bytes 4194304 | tf_op jit(solution)/shard_map/all_to_all | solution.py:165
  242.2 12.1 %all-gather.6.cloned.1.call-done = bf16[32,32,2048]{2,1,0:T(8,128)(2,1)} async-done(((bf16[16,32,2048]{2,1,0:T(8,128)(2,1)}), bf16[32,32,2048]{2,1,0:T(8,128)(2,1)}) %all-gather.6.cloned.1.call-update) | async-done | bytes 4194320 | tf_op jit(solution)/shard_map/all_gather | solution.py:167
  254.3 5.3 %fusion.24 = f32[1024,512]{1,0:T(8,128)S(1)} fusion(bf16[1024,2048]{1,0:T(8,128)(2,1)} %bitcast.88, bf16[1,2048,512]{2,1,0:T(8,128)(2,1)} %param.32), kind=kOutput, calls=%fused_computation.31 | convolution fusion | flops 2147483648 | bytes 8388608 | tf_op jit(solution)/shard_map/dot_general | solution.py:170
  259.6 2.7 multiply_convert_fusion
  262.3 4.3 %convolution_convert_fusion.2 = bf16[32,32,2048]{2,1,0:T(8,128)(2,1)} fusion(bf16[32,32,512]{2,1,0:T(8,128)(2,1)S(1)} %bitcast.90, bf16[1,512,2048]{2,1,0:T(8,128)(2,1)S(1)} %copy-done.20), kind=kOutput, calls=%fused_computation.28 | convolution fusion | flops 2149580800 | bytes 7340032 | tf_op jit(solution)/shard_map/dot_general | solution.py:172
  266.6 13.3 %reduce-scatter.2.cloned.1.call-done = bf16[16,32,2048]{2,1,0:T(8,128)(2,1)} async-done(((bf16[32,32,2048]{2,1,0:T(8,128)(2,1)}), bf16[16,32,2048]{2,1,0:T(8,128)(2,1)}) %reduce-scatter.2.cloned.1.call-update) | async-done | bytes 2097168 | tf_op jit(solution)/shard_map/reduce_scatter | solution.py:175
  280.0 7.1 %all-to-all-start.2 = ((bf16[16,32,2048]{2,1,0:T(8,128)(2,1)}), bf16[16,32,2048]{2,1,0:T(8,128)(2,1)}, u32[]{:S(2)}, u32[]{:S(2)}) async-start(bf16[16,32,2048]{2,1,0:T(8,128)(2,1)} %reduce-scatter.2.cloned.1.call-done), calls=%async_computation.3 | async-start | bytes 4194304 | tf_op jit(solution)/shard_map/all_to_all | solution.py:178
  287.4 43.0 %all-to-all-done.2 = bf16[16,32,2048]{2,1,0:T(8,128)(2,1)} async-done(((bf16[16,32,2048]{2,1,0:T(8,128)(2,1)}), bf16[16,32,2048]{2,1,0:T(8,128)(2,1)}, u32[]{:S(2)}, u32[]{:S(2)}) %all-to-all-start.2) | async-done | bytes 2097184 | tf_op jit(solution)/shard_map/all_to_all | solution.py:178
  330.4 5.2 %gather_fusion = bf16[256,2048]{1,0:T(8,128)(2,1)} fusion(bf16[512,2048]{1,0:T(8,128)(2,1)} %bitcast.21, s32[1024]{0:T(1024)S(1)} %pad_clamp_fusion), kind=kCustom, calls=%fused_computation | custom fusion | bytes 2098176 | tf_op jit(solution)/shard_map/gather | solution.py:179
  335.6 3.4 reshape.225
  339.0 4.9 %multiply_reduce_fusion = f32[128,2048]{1,0:T(8,128)S(1)} fusion(f32[128,2,2048]{2,1,0:T(2,128)} %reshape.225, f32[128,2]{1,0:T(8,128)S(1)} %copy.46), kind=kLoop, calls=%fused_computation.35 | loop fusion | flops 786432 | bytes 3146752 | tf_op jit(solution)/shard_map/reduce_sum | solution.py:180
  343.9 0.9 fusion.33
  (111 shorter events, 11.7 us)
Async XLA Ops:
  6.5 157.3 %copy-start = (bf16[768,2048]{1,0:T(8,128)(2,1)S(1)}, bf16[768,2048]{1,0:T(8,128)(2,1)}, u32[]{:S(2)}) copy-start(bf16[768,2048]{1,0:T(8,128)(2,1)} %param.26) | copy-start | bytes 9437188
  6.5 94.0 %all-gather.4.cloned.1.call-start = ((), (), s32[]{:S(2)}) async-start(), calls=%async_computation.4 | async-start | bytes 2228224 | tf_op jit(solution)/shard_map/all_gather | solution.py:104
  7.3 247.0 %all-gather.6.cloned.1.call-start = ((), (), s32[]{:S(2)}) async-start(), calls=%async_computation.5 | async-start | bytes 6291456 | tf_op jit(solution)/shard_map/all_gather | solution.py:167
  11.1 0.6 copy-start.13
  101.3 0.6 copy-start.8
  106.9 2.9 copy-start.10
  106.9 2.9 copy-start.9
  106.9 2.9 copy-start.11
  106.9 2.9 copy-start.12
  106.9 3.1 copy-start.3
  110.9 0.9 copy-start.4
  114.7 0.6 copy-start.8
  121.0 0.6 copy-start.8
  127.3 0.6 copy-start.8
  133.7 0.6 copy-start.8
  140.0 0.6 copy-start.8
  146.3 0.6 copy-start.8
  152.7 0.6 copy-start.8
  163.9 1.0 copy-start.5
  163.9 1.0 copy-start.15
  164.5 1.4 copy-start.6
  164.6 1.4 copy-start.16
  165.1 0.8 copy-start.1
  242.1 37.9 %reduce-scatter.2.cloned.1.call-start = ((), (), s32[]{:S(2)}) async-start(), calls=%async_computation.6 | async-start | bytes 6291456 | tf_op jit(solution)/shard_map/reduce_scatter | solution.py:175
  254.3 5.3 %copy-start.18 = (bf16[32,32,2048]{2,1,0:T(8,128)(2,1)S(1)}, bf16[32,32,2048]{2,1,0:T(8,128)(2,1)}, u32[]{:S(2)}) copy-start(bf16[32,32,2048]{2,1,0:T(8,128)(2,1)} %all-gather.6.cloned.1.call-done) | copy-start | bytes 12582916
  254.3 5.3 %copy-start.19 = (bf16[1,2048,512]{2,1,0:T(8,128)(2,1)S(1)}, bf16[1,2048,512]{2,1,0:T(8,128)(2,1)}, u32[]{:S(2)}) copy-start(bf16[1,2048,512]{2,1,0:T(8,128)(2,1)} %param.31) | copy-start | bytes 6291460
  259.6 2.7 copy-start.20
  266.6 20.5 %copy-start.7 = (s32[128,2]{1,0:T(8,128)S(1)}, s32[128,2]{1,0:T(8,128)}, u32[]{:S(2)}) copy-start(s32[128,2]{1,0:T(8,128)} %get-tuple-element.385) | copy-start | bytes 3076
  266.6 20.7 %copy-start.17 = (f32[128,2]{0,1:T(2,128)S(1)}, f32[128,2]{0,1:T(2,128)}, u32[]{:S(2)}) copy-start(f32[128,2]{0,1:T(2,128)} %param.30) | copy-start | bytes 3076
  266.6 20.8 %copy-start.14 = (s32[256]{0:T(256)S(1)}, s32[256]{0:T(256)}, u32[]{:S(2)}) copy-start(s32[256]{0:T(256)} %copy-done.13) | copy-start | bytes 3076
  280.0 50.5 %all-to-all-start.2 = ((bf16[16,32,2048]{2,1,0:T(8,128)(2,1)}), bf16[16,32,2048]{2,1,0:T(8,128)(2,1)}, u32[]{:S(2)}, u32[]{:S(2)}) async-start(bf16[16,32,2048]{2,1,0:T(8,128)(2,1)} %reduce-scatter.2.cloned.1.call-done), calls=%async_computation.3 | async-start | bytes 4194304 | tf_op jit(solution)/shard_map/all_to_all | solution.py:178
  339.0 4.9 %copy-start.2 = (bf16[128,2048]{1,0:T(8,128)(2,1)S(1)}, bf16[128,2048]{1,0:T(8,128)(2,1)}, u32[]{:S(2)}) copy-start(bf16[128,2048]{1,0:T(8,128)(2,1)} %copy-done.1) | copy-start | bytes 1572868
Sparse Core Ops, SparseCore 0:
  10.1 64.8 all-gather.3
  242.2 11.9 all-gather.5
  266.7 13.2 reduce-scatter.1
where the time goes:
time: 357 us; the launch traced here: 351 us
  blocking collectives  164 us (46%)
  waiting for transfers between devices  69.2 us (19%)
  local copies, waits for them, and re-layouts  50.6 us (14%)
  matrix products  19.4 us (5%)
  loops' own time  15.3 us (4%)
  between operations  13.4 us (4%)
  other arithmetic  12.7 us (4%)
  starting transfers between devices  7.22 us (2%)
    all_to_all x1, blocking collectives, local(): lax.all_to_all(buffer, 'sp', split_axis=0, concat_axis=0, tiled=True)  75.4 us
    all_gather x1, blocking collectives, local(): lax.all_gather(doc_ids, 'sp', axis=0, tiled=True)  44.9 us
    all_to_all x1, waiting for transfers between devices, local(): lax.all_to_all(summed, 'sp', split_axis=0, concat_axis=0, tiled=True)  43 us
    all_gather x1, blocking collectives, local(): lax.all_gather(key_rot, 'sp', axis=0, tiled=True)  39.4 us
    slice x24, local copies, waits for them, and re-layouts, one_block(): active = (first_row <= query_pos[-1]) & (sliced[-1][-1] >= doc_ids[0])  24.7 us
    another operation x1, loops' own time, local(): running = lax.fori_loop(0, row_count // block_rows, one_block, initial)  15 us
    reduce_scatter x1, waiting for transfers between devices, local(): lax.psum_scatter(partial_value.astype(jnp.bfloat16), 'tp', scatter_dimens...  13.3 us
    all_gather x1, waiting for transfers between devices, local(): both_halves = lax.all_gather(arrived, 'tp', axis=0, tiled=True)  12.1 us
  transfers between devices with their start and end apart: 4, of which 3 were waited for; matrix products, arithmetic and copies ran while one was open for 2% of the time, Pallas kernels for 0%

commit v1 on v0

v1 whole, which is shorter than its diff:
```python
import functools
import math

import jax
import jax.numpy as jnp
from jax import lax
from jax.experimental import pallas as pl
from jax.experimental.pallas import tpu as pltpu
from jax.sharding import PartitionSpec as P

UNROTATED_DIM = 64
ROPE = 32
VALUE_ENTRIES = 64
GROUPS = 4
HEAD_LANES = 128

rope_base = 10000.0
epsilon = 1e-06


def angles_of(positions):
    half_width = ROPE // 2
    frequency = rope_base ** (-jnp.arange(half_width, dtype=jnp.float32) / half_width)
    angles = positions.astype(jnp.float32)[:, None] * frequency[None, :]
    return jnp.cos(angles), jnp.sin(angles)


def rms_scale(source, gain):
    return source * lax.rsqrt(jnp.mean(source * source, axis=-1, keepdims=True) + epsilon) * gain


def attention_kernel(
    heads, block, lo_ref, query_ref, table_ref, span_ref, packed_ref, wk_ref, wv_ref, out_ref,
    turned, high, total, acc,
):
    rows = query_ref.shape[0]
    width = query_ref.shape[1]
    rank = wk_ref.shape[0]
    per_head = UNROTATED_DIM + ROPE
    cosine = table_ref[:, :HEAD_LANES]
    sine = table_ref[:, HEAD_LANES:]
    for h in range(heads):
        first = h * per_head // 128 * 128
        last = min(-(-(h + 1) * per_head // 128) * 128, width)
        window = query_ref[:, first:last]
        shape = (last - first, HEAD_LANES)
        source = lax.broadcasted_iota(jnp.int32, shape, 0) + (first - h * per_head)
        lane = lax.broadcasted_iota(jnp.int32, shape, 1)
        half = ROPE // 2
        plain = jnp.where((source == lane) & (lane < per_head), 1.0, 0.0).astype(jnp.bfloat16)
        upper = (lane >= UNROTATED_DIM) & (lane < UNROTATED_DIM + half) & (source == lane + half)
        lower = (lane >= UNROTATED_DIM + half) & (lane < per_head) & (source == lane - half)
        crossed = (jnp.where(lower, 1.0, 0.0) - jnp.where(upper, 1.0, 0.0)).astype(jnp.bfloat16)
        straight = jnp.dot(window, plain, preferred_element_type=jnp.float32)
        swapped = jnp.dot(window, crossed, preferred_element_type=jnp.float32)
        turned[h] = (straight * cosine + swapped * sine).astype(jnp.bfloat16)
    high[...] = jnp.full(high.shape, -1e30, jnp.float32)
    total[...] = jnp.zeros(total.shape, jnp.float32)
    acc[...] = jnp.zeros(acc.shape, jnp.float32)
    span_first = span_ref[0:1, :]
    span_last = span_ref[1:2, :]
    scale = per_head ** (-0.5)

    def step(number, carry):
        base = pl.multiple_of(number * block, block)
        latent = packed_ref[pl.ds(base, block), :rank]
        extra = packed_ref[pl.ds(base, block), rank:]
        position = base + lax.broadcasted_iota(jnp.int32, (block, rows), 0)
        live = (position >= span_first) & (position <= span_last)
        values_t = lax.dot_general(
            wv_ref[...], latent, (((0,), (1,)), ((), ())), preferred_element_type=jnp.float32
        ).astype(jnp.bfloat16)
        for h in range(heads):
            keys = jnp.dot(
                latent, wk_ref[:, h * HEAD_LANES : (h + 1) * HEAD_LANES],
                preferred_element_type=jnp.float32,
            ).astype(jnp.bfloat16) + extra
            scores = lax.dot_general(
                keys, turned[h], (((1,), (1,)), ((), ())), preferred_element_type=jnp.float32
            ) * scale
            scores = jnp.where(live, scores, -1e30)
            old = high[h : h + 1, :]
            new = jnp.maximum(old, jnp.max(scores, axis=0, keepdims=True))
            weights = jnp.where(live, jnp.exp(scores - new), 0.0)
            factor = jnp.exp(old - new)
            high[h : h + 1, :] = new
            total[h : h + 1, :] = total[h : h + 1, :] * factor + jnp.sum(
                weights, axis=0, keepdims=True
            )
            acc[h] = acc[h] * factor + jnp.dot(
                values_t[h * VALUE_ENTRIES : (h + 1) * VALUE_ENTRIES],
                weights.astype(jnp.bfloat16),
                preferred_element_type=jnp.float32,
            )
        return carry

    lax.fori_loop(lo_ref[0], lo_ref[1], step, 0)
    for h in range(heads):
        out_ref[h * VALUE_ENTRIES : (h + 1) * VALUE_ENTRIES, :] = (
            acc[h] / total[h : h + 1, :]
        ).astype(jnp.bfloat16)


def attend(queries, packed, doc_ids, latent_to_key, latent_to_value, positions, cosine, sine):
    rows = queries.shape[0]
    heads = queries.shape[1] // (UNROTATED_DIM + ROPE)
    rank = latent_to_key.shape[0]
    count = packed.shape[0]
    docs = packed[:, rank + UNROTATED_DIM + ROPE].astype(jnp.int32)
    starts = jnp.sum((docs[:, None] < doc_ids[None, :]).astype(jnp.int32), axis=0)
    block = math.gcd(count, 256)
    bounds = jnp.stack([starts[0] // block, positions[-1] // block + 1]).astype(jnp.int32)
    span = jnp.stack([starts, positions])
    one, none = jnp.ones((rows, UNROTATED_DIM)), jnp.zeros((rows, HEAD_LANES - UNROTATED_DIM - ROPE))
    table = jnp.concatenate(
        [one, cosine, cosine, none, 0.0 * one, sine, sine, none], axis=1
    ).astype(jnp.float32)
    wk = jnp.pad(
        latent_to_key.reshape(rank, heads, UNROTATED_DIM),
        ((0, 0), (0, 0), (0, HEAD_LANES - UNROTATED_DIM)),
    ).reshape(rank, heads * HEAD_LANES)
    vmem = pl.BlockSpec(memory_space=pltpu.VMEM)
    out = pl.pallas_call(
        functools.partial(attention_kernel, heads, block),
        out_shape=jax.ShapeDtypeStruct((heads * VALUE_ENTRIES, rows), jnp.bfloat16),
        in_specs=[pl.BlockSpec(memory_space=pltpu.SMEM)] + [vmem] * 6,
        out_specs=vmem,
        scratch_shapes=[
            pltpu.VMEM((heads, rows, HEAD_LANES), jnp.bfloat16),
            pltpu.VMEM((heads, rows), jnp.float32),
            pltpu.VMEM((heads, rows), jnp.float32),
            pltpu.VMEM((heads, VALUE_ENTRIES, rows), jnp.float32),
        ],
        compiler_params=pltpu.CompilerParams(vmem_limit_bytes=40 * 1024 * 1024),
        name="attend",
    )(bounds, queries, table, span, packed, wk, latent_to_value)
    return out.T


def local(
    residual,
    queries,
    latent,
    rope_key,
    doc_ids,
    latent_to_key,
    latent_to_value,
    out_proj,
    mix_gain,
    moe_gain,
    expert_ids,
    route_weight,
    gate_weight,
    up_weight,
    down_weight,
):
    local_rows = queries.shape[0]
    positions = lax.axis_index("sp") * local_rows + jnp.arange(local_rows, dtype=jnp.int32)
    cosine, sine = angles_of(positions)
    half = ROPE // 2
    upper, lower = rope_key[:, :half].astype(jnp.float32), rope_key[:, half:].astype(jnp.float32)
    key_rot = jnp.concatenate(
        [upper * cosine - lower * sine, lower * cosine + upper * sine], axis=1
    ).astype(jnp.bfloat16)
    own = jnp.concatenate(
        [
            latent,
            jnp.zeros((local_rows, UNROTATED_DIM), jnp.bfloat16),
            key_rot,
            doc_ids.astype(jnp.bfloat16)[:, None],
            jnp.zeros((local_rows, HEAD_LANES - UNROTATED_DIM - ROPE - 1), jnp.bfloat16),
        ],
        axis=1,
    )
    packed = lax.all_gather(own, "sp", axis=0, tiled=True)
    attended = attend(
        queries, packed, doc_ids, latent_to_key, latent_to_value, positions, cosine, sine
    )
    gathered = lax.all_to_all(attended, "tp", split_axis=0, concat_axis=1, tiled=True)
    mix = jnp.dot(gathered, out_proj, preferred_element_type=jnp.float32)
    branch = rms_scale(mix, mix_gain)
    middle = lax.optimization_barrier((residual.astype(jnp.float32) + branch).astype(jnp.bfloat16))
    normed = rms_scale(middle.astype(jnp.float32), moe_gain).astype(jnp.bfloat16)
    row_count = normed.shape[0]
    width = normed.shape[1]
    top_count = expert_ids.shape[1]
    expert_count = lax.axis_size("sp")
    capacity = row_count // (expert_count // GROUPS)
    flat_ids = expert_ids.reshape(-1)
    onehot = (flat_ids[:, None] == jnp.arange(expert_count, dtype=jnp.int32)[None, :]).astype(
        jnp.int32
    )
    earlier = jnp.cumsum(onehot, axis=0) - onehot
    slot_rank = jnp.sum(earlier * onehot, axis=1)
    slot_ids = (flat_ids * capacity + slot_rank).reshape(row_count, top_count)
    matches = (
        slot_ids[:, :, None]
        == jnp.arange(expert_count * capacity, dtype=jnp.int32)[None, None, :]
    )
    chooser = jnp.any(matches, axis=1).astype(jnp.bfloat16)
    buffer = lax.dot_general(
        chooser, normed, (((0,), (0,)), ((), ())), preferred_element_type=jnp.float32
    ).astype(jnp.bfloat16)
    buffer = buffer.reshape(expert_count, capacity, width)
    arrived = lax.all_to_all(buffer, "sp", split_axis=0, concat_axis=0, tiled=True)
    both_halves = lax.all_gather(arrived, "tp", axis=0, tiled=True)
    flat_rows = both_halves.reshape(-1, width)
    gate_out = jnp.dot(flat_rows, gate_weight[0], preferred_element_type=jnp.float32)
    upward = jnp.dot(flat_rows, up_weight[0], preferred_element_type=jnp.float32)
    hidden = (jax.nn.silu(gate_out) * upward).astype(jnp.bfloat16)
    partial_value = jnp.dot(hidden, down_weight[0], preferred_element_type=jnp.float32).reshape(
        both_halves.shape
    )
    summed = lax.psum_scatter(
        partial_value.astype(jnp.bfloat16), "tp", scatter_dimension=0, tiled=True
    )
    returned = lax.all_to_all(summed, "sp", split_axis=0, concat_axis=0, tiled=True)
    share = jnp.sum(jnp.where(matches, route_weight[:, :, None], 0.0), axis=1)
    coarse = share.astype(jnp.bfloat16)
    fine = (share - coarse.astype(jnp.float32)).astype(jnp.bfloat16)
    flat = returned.reshape(-1, width)
    expert_mix = jnp.dot(coarse, flat, preferred_element_type=jnp.float32) + jnp.dot(
        fine, flat, preferred_element_type=jnp.float32
    )
    return (middle.astype(jnp.float32) + expert_mix).astype(jnp.bfloat16)


def solution(mesh):
    in_specs = (
        P(("sp", "tp"), None),
        P("sp", "tp"),
        P("sp", None),
        P("sp", None),
        P("sp"),
        P(None, "tp"),
        P(None, "tp"),
        P(),
        P(),
        P(),
        P(("sp", "tp"), None),
        P(("sp", "tp"), None),
        P("sp", None, "tp"),
        P("sp", None, "tp"),
        P("sp", "tp", None),
    )
    out_specs = P(("sp", "tp"), None)
    return jax.shard_map(local, mesh=mesh, in_specs=in_specs, out_specs=out_specs, check_vma=False)
```

time: 357 us -> 279 us (0.78)
  blocking collectives: 164 us -> 74.1 us
  waiting for transfers between devices: 69.2 us -> 116 us
  local copies, waits for them, and re-layouts: 50.6 us -> 23.5 us
  loops' own time: 15.3 us -> 0 us
  between operations: 13.4 us -> 18.2 us
    all_gather x2 -> x0, blocking collectives: 84.3 us -> none  [the longest x1 44.9 us: local(): lax.all_gather(doc_ids, 'sp', axis=0, tiled=True)]
    all_gather x1, waiting for transfers between devices: 0.01 us -> 47.1 us  [local(): packed = lax.all_gather(own, 'sp', axis=0, tiled=True)]
    slice x25 -> x4, local copies, waits for them, and re-layouts: 26.3 us -> 2 us  [the longest x24 24.7 us: one_block(): active = (first_row <= query_pos[-1]) & (sliced[-1][-1] >= doc_ids[0])]
    another operation x9 -> x0, loops' own time: 15.3 us -> none  [the longest x1 15 us: local(): running = lax.fori_loop(0, row_count // block_rows, one_block, initial)]
    unnamed x30 -> x35, local copies, waits for them, and re-layouts: 2.63 us -> 9.41 us
    dynamic_slice x8 -> x0, local copies, waits for them, and re-layouts: 6.04 us -> none  [one_block(): lax.dynamic_slice_in_dim(member, first_row, block_rows, 0)]
    gather x1 -> x0, local copies, waits for them, and re-layouts: 5.2 us -> none  [local(): picked = returned.reshape(-1, D)[slot_ids.reshape(-1)].astype(jnp.float32)]
    all_to_all x1, blocking collectives: 75.4 us -> 70.2 us  [local(): lax.all_to_all(buffer, 'sp', split_axis=0, concat_axis=0, tiled=True)]
  transfers between devices with their start and end apart: 4 -> 4, of which waited for: 3 -> 4; matrix products, arithmetic and copies ran while one was open for 2% -> 8% of each run, Pallas kernels for 0% -> 0%
where the time goes in v1:
time: 279 us; the launch traced here: 274 us
  waiting for transfers between devices  116 us (42%)
  blocking collectives  74.1 us (27%)
  local copies, waits for them, and re-layouts  23.5 us (8%)
  matrix products  18.7 us (7%)
  between operations  18.2 us (7%)
  other arithmetic  13.4 us (5%)
  starting transfers between devices  7.24 us (3%)
  Pallas kernels  3.31 us (1%)
    all_to_all x1, blocking collectives, local(): lax.all_to_all(buffer, 'sp', split_axis=0, concat_axis=0, tiled=True)  70.2 us
    all_gather x1, waiting for transfers between devices, local(): packed = lax.all_gather(own, 'sp', axis=0, tiled=True)  47.1 us
    all_to_all x1, waiting for transfers between devices, local(): lax.all_to_all(summed, 'sp', split_axis=0, concat_axis=0, tiled=True)  43.2 us
    reduce_scatter x1, waiting for transfers between devices, local(): lax.psum_scatter(partial_value.astype(jnp.bfloat16), 'tp', scatter_dimens...  13.3 us
    all_gather x1, waiting for transfers between devices, local(): both_halves = lax.all_gather(arrived, 'tp', axis=0, tiled=True)  11.9 us
    unnamed x35, local copies, waits for them, and re-layouts  9.41 us
    all_to_all x1, starting transfers between devices, local(): lax.all_to_all(summed, 'sp', split_axis=0, concat_axis=0, tiled=True)  6.98 us
  transfers between devices with their start and end apart: 4, of which 4 were waited for; matrix products, arithmetic and copies ran while one was open for 8% of the time, Pallas kernels for 0%

profile of v1, /device:TPU:0, one launch (start us, length us, event | category | flops | bytes accessed | tf_op | source)
XLA Modules:
  0.0 273.9 jit_solution(13480343562032362768)
XLA Ops:
  6.6 0.9 slice_convert_fusion
  7.4 0.1 copy.60
  7.5 0.1 copy.61
  7.7 0.7 convert_element_type.70
  8.3 0.1 broadcast_in_dim.45
  8.4 1.3 fusion.19
  9.8 1.8 concatenate.9
  11.5 0.0 all-gather.3.cloned.1.call-update
  11.6 0.0 all-gather.5.cloned.1.call-start
  11.6 0.6 slice.25
  13.5 0.8 copy.68
  14.3 0.1 eq.42
  14.4 0.7 eq.38
  16.4 1.1 copy.64
  17.5 0.8 pad.4
  18.3 1.2 copy.66.wk_ref
  19.4 1.9 copy.65.query_ref
  21.3 0.6 fusion.26
  21.9 1.3 reduce-window.6
  23.2 0.8 slice_reduce_fusion
  23.9 1.3 reduce-window.9
  25.2 0.7 slice.27
  25.9 1.3 fusion.25
  27.2 1.5 reduce_sum.50
  28.7 0.9 copy.71
  29.6 0.7 broadcast_in_dim.41
  30.2 0.7 broadcast_in_dim.42
  30.9 0.7 mul.95
  31.6 2.3 concatenate.10.table_ref
  33.9 0.7 multiply_add_fusion
  34.5 0.7 fusion.15
  35.3 47.1 %all-gather.3.cloned.1.call-done.packed_ref = bf16[4096,384]{1,0:T(8,128)(2,1)} async-done(((bf16[256,384]{1,0:T(8,128)(2,1)}), bf16[4096,384]{1,0:T(8,128)(2,1)}) %all-gather.3.cloned.1.call-update) | async-done | bytes 3145744 | tf_op jit(solution)/shard_map/all_gather | solution.py:175
  82.3 2.1 convert_reduce_fusion.1
  84.5 1.9 convert_reduce_fusion
  86.3 0.5 slice.24
  89.1 0.1 pad_add_fusion.1.lo_ref
  89.2 1.9 copy-done.1
  91.1 1.0 copy-done.2
  92.1 0.9 copy-done.3
  93.0 0.9 copy-done.4
  93.9 3.3 %attend.1 = bf16[384,256]{1,0:T(8,128)(2,1)S(1)} custom-call(s32[2]{0:T(128)S(1)} %pad_add_fusion.1.lo_ref, bf16[256,576]{1,0:T(8,128)(2,1)S(1)} %copy-done.2, f32[256,256]{1,0:T(8,128)S(1)} %copy-done.3, s32[2,256]{1,0:T(2,128)S(1)} %pad_add_fusion.span_ref, bf16[4096,384]{1,0:T(8,128)(2,1)S(1)} %copy-done.1, bf16[256,768]{1,0:T(8,128)(2,1)S(1)} %copy.66.wk_ref, ...), custom_call_target="tpu_custom_call" | custom-call | tf_op jit(solution)/shard_map/attend/pallas_call | solution.py:123
  97.3 3.9 %all_to_all.29 = bf16[2,128,384]{1,2,0:T(8,128)(2,1)S(1)} all-to-all(bf16[2,128,384]{1,2,0:T(8,128)(2,1)S(1)} %copy_bitcast_fusion), channel_id=1, replica_groups=mesh['sp'=16,'tp'=2] {'tp'}, dimensions={0} | all-to-all | bytes 393216 | tf_op jit(solution)/shard_map/all_to_all | solution.py:179
  101.2 0.7 multiply_reduce_fusion
  101.9 0.0 copy-start.10
  101.9 0.3 copy-done.7
  102.2 0.2 add_convert_fusion
  102.4 0.0 copy-start.5
  102.5 0.2 fusion.9
  102.7 0.6 copy-done.5
  103.3 0.8 convolution_convert_fusion.1
  104.1 70.2 %all_to_all.30 = bf16[16,32,2048]{2,1,0:T(8,128)(2,1)} all-to-all(bf16[16,32,2048]{2,1,0:T(8,128)(2,1)S(1)} %bitcast.59), channel_id=1, replica_groups=mesh['sp'=16,'tp'=2] {'sp'}, dimensions={0} | all-to-all | bytes 4194304 | tf_op jit(solution)/shard_map/all_to_all | solution.py:205
  174.3 0.0 all-gather.5.cloned.1.call-update
  174.3 0.2 reduce-scatter.2.cloned.1.call-start
  174.6 11.9 %all-gather.5.cloned.1.call-done = bf16[32,32,2048]{2,1,0:T(8,128)(2,1)} async-done(((bf16[16,32,2048]{2,1,0:T(8,128)(2,1)}), bf16[32,32,2048]{2,1,0:T(8,128)(2,1)}) %all-gather.5.cloned.1.call-update) | async-done | bytes 4194320 | tf_op jit(solution)/shard_map/all_gather | solution.py:206
  186.5 5.3 %fusion.3 = f32[1024,512]{1,0:T(8,128)S(1)} fusion(bf16[1024,2048]{1,0:T(8,128)(2,1)} %bitcast.64, bf16[1,2048,512]{2,1,0:T(8,128)(2,1)} %param.28), kind=kOutput, calls=%fused_computation.7 | convolution fusion | flops 2147483648 | bytes 8388608 | tf_op jit(solution)/shard_map/dot_general | solution.py:209
  191.8 2.7 multiply_convert_fusion
  194.5 4.3 %convolution_convert_fusion = bf16[32,32,2048]{2,1,0:T(8,128)(2,1)} fusion(bf16[32,32,512]{2,1,0:T(8,128)(2,1)S(1)} %bitcast.66, bf16[1,512,2048]{2,1,0:T(8,128)(2,1)S(1)} %copy-done.15), kind=kOutput, calls=%fused_computation.1 | convolution fusion | flops 2149580800 | bytes 7340032 | tf_op jit(solution)/shard_map/dot_general | solution.py:211
  198.8 0.0 reduce-scatter.2.cloned.1.call-update
  198.8 13.3 %reduce-scatter.2.cloned.1.call-done = bf16[16,32,2048]{2,1,0:T(8,128)(2,1)} async-done(((bf16[32,32,2048]{2,1,0:T(8,128)(2,1)}), bf16[16,32,2048]{2,1,0:T(8,128)(2,1)}) %reduce-scatter.2.cloned.1.call-update) | async-done | bytes 2097168 | tf_op jit(solution)/shard_map/reduce_scatter | solution.py:214
  212.1 7.0 %all-to-all-start.2 = ((bf16[16,32,2048]{2,1,0:T(8,128)(2,1)}), bf16[16,32,2048]{2,1,0:T(8,128)(2,1)}, u32[]{:S(2)}, u32[]{:S(2)}) async-start(bf16[16,32,2048]{2,1,0:T(8,128)(2,1)} %reduce-scatter.2.cloned.1.call-done), calls=%async_computation.3 | async-start | bytes 4194304 | tf_op jit(solution)/shard_map/all_to_all | solution.py:217
  219.1 0.1 select_reduce_fusion
  219.3 43.2 %all-to-all-done.2 = bf16[16,32,2048]{2,1,0:T(8,128)(2,1)} async-done(((bf16[16,32,2048]{2,1,0:T(8,128)(2,1)}), bf16[16,32,2048]{2,1,0:T(8,128)(2,1)}, u32[]{:S(2)}, u32[]{:S(2)}) %all-to-all-start.2) | async-done | bytes 2097184 | tf_op jit(solution)/shard_map/all_to_all | solution.py:217
  262.4 2.1 fusion.21
  264.6 2.8 %fusion.1 = bf16[128,2048]{1,0:T(8,128)(2,1)} fusion(f32[128,2048]{1,0:T(8,128)S(1)} %fusion.21, bf16[512,2048]{1,0:T(8,128)(2,1)} %bitcast.18, bf16[128,2048]{1,0:T(8,128)(2,1)S(1)} %copy-done.6, f32[128,512]{1,0:T(8,128)S(1)} %select_reduce_fusion), kind=kOutput, calls=%fused_computation.5 | convolution fusion | flops 269746176 | bytes 4456448 | tf_op jit(solution)/shard_map/dot_general | solution.py:222
  (34 shorter events, 0.1 us)
Async XLA Ops:
  6.5 94.6 %copy-start = (bf16[768,2048]{1,0:T(8,128)(2,1)S(1)}, bf16[768,2048]{1,0:T(8,128)(2,1)}, u32[]{:S(2)}) copy-start(bf16[768,2048]{1,0:T(8,128)(2,1)} %param.22) | copy-start | bytes 9437188
  6.5 75.8 %all-gather.3.cloned.1.call-start = ((), (), s32[]{:S(2)}) async-start(), calls=%async_computation.4 | async-start | bytes 3342336 | tf_op jit(solution)/shard_map/all_gather | solution.py:175
  11.6 174.9 %all-gather.5.cloned.1.call-start = ((), (), s32[]{:S(2)}) async-start(), calls=%async_computation.5 | async-start | bytes 6291456 | tf_op jit(solution)/shard_map/all_gather | solution.py:206
  27.2 57.3 %copy-start.12 = (s32[256]{0:T(256)S(1)}, s32[256]{0:T(256)}, u32[]{:S(2)}) copy-start(s32[256]{0:T(256)} %param.19) | copy-start | bytes 3076
  89.2 1.9 copy-start.1
  91.1 1.0 copy-start.2
  92.1 0.9 copy-start.3
  93.0 0.9 copy-start.4
  101.2 1.0 copy-start.7
  101.2 1.0 copy-start.9
  101.9 1.4 copy-start.8
  101.9 1.4 copy-start.10
  102.4 0.8 copy-start.5
  174.3 37.8 %reduce-scatter.2.cloned.1.call-start = ((), (), s32[]{:S(2)}) async-start(), calls=%async_computation.6 | async-start | bytes 6291456 | tf_op jit(solution)/shard_map/reduce_scatter | solution.py:214
  186.5 5.3 %copy-start.13 = (bf16[32,32,2048]{2,1,0:T(8,128)(2,1)S(1)}, bf16[32,32,2048]{2,1,0:T(8,128)(2,1)}, u32[]{:S(2)}) copy-start(bf16[32,32,2048]{2,1,0:T(8,128)(2,1)} %all-gather.5.cloned.1.call-done) | copy-start | bytes 12582916
  186.5 5.3 %copy-start.14 = (bf16[1,2048,512]{2,1,0:T(8,128)(2,1)S(1)}, bf16[1,2048,512]{2,1,0:T(8,128)(2,1)}, u32[]{:S(2)}) copy-start(bf16[1,2048,512]{2,1,0:T(8,128)(2,1)} %param.27) | copy-start | bytes 6291460
  191.8 2.7 copy-start.15
  198.8 20.3 %copy-start.11 = (f32[128,2]{0,1:T(2,128)S(1)}, f32[128,2]{0,1:T(2,128)}, u32[]{:S(2)}) copy-start(f32[128,2]{0,1:T(2,128)} %param.26) | copy-start | bytes 3076
  212.1 50.3 %all-to-all-start.2 = ((bf16[16,32,2048]{2,1,0:T(8,128)(2,1)}), bf16[16,32,2048]{2,1,0:T(8,128)(2,1)}, u32[]{:S(2)}, u32[]{:S(2)}) async-start(bf16[16,32,2048]{2,1,0:T(8,128)(2,1)} %reduce-scatter.2.cloned.1.call-done), calls=%async_computation.3 | async-start | bytes 4194304 | tf_op jit(solution)/shard_map/all_to_all | solution.py:217
  262.4 2.1 copy-start.6
Sparse Core Ops, SparseCore 0:
  11.7 70.5 all-gather.2
  174.5 11.9 all-gather.4
  198.9 13.1 reduce-scatter.1

commit v2 on v1

--- a/solution.py
+++ b/solution.py
@@ -13,6 +13,7 @@
 VALUE_ENTRIES = 64
 GROUPS = 4
 HEAD_LANES = 128
+MESH = pl.DeviceIdType.MESH
 
 rope_base = 10000.0
 epsilon = 1e-06
@@ -137,6 +138,237 @@
     return out.T
 
 
+def greet(groups, plane):
+    index, core = lax.axis_index("sp"), lax.axis_index("tp")
+    level, place = index // plane, lax.rem(index, plane)
+    barrier = pltpu.get_barrier_semaphore()
+    peers = [(lax.rem(level + d, groups) * plane + place, core) for d in range(1, groups)]
+    peers += [(level * plane + lax.rem(place + d, plane), core) for d in range(1, plane)]
+    peers += [(index, 1 - core)]
+    for peer in peers:
+        pl.semaphore_signal(barrier, inc=1, device_id=peer, device_id_type=MESH)
+    pl.semaphore_wait(barrier, len(peers))
+    return index, core, level, place
+
+
+def remote(source, target, send_sem, recv_sem, peer):
+    return pltpu.make_async_remote_copy(
+        src_ref=source, dst_ref=target, send_sem=send_sem, recv_sem=recv_sem,
+        device_id=peer, device_id_type=MESH,
+    )
+
+
+def level_order(groups):
+    return sorted(range(groups), key=lambda d: min(d, groups - d))
+
+
+def dispatch_kernel(
+    groups, plane, capacity, rows_ref, meta_ref, out_ref, metas_ref,
+    landed, spread, z_send, z_recv, m_send, m_recv, p_send, p_recv, t_send, t_recv, own_sem,
+):
+    index, core, level, place = greet(groups, plane)
+    started = []
+    for d in sorted(range(1, groups), key=lambda d: -min(d, groups - d)):
+        other = lax.rem(level + d, groups)
+        peer = (other * plane + place, core)
+        first = remote(
+            meta_ref.at[other], metas_ref.at[level], m_send.at[d], m_recv.at[level], peer
+        )
+        second = remote(
+            rows_ref.at[other], landed.at[level], z_send.at[d], z_recv.at[level], peer
+        )
+        first.start()
+        second.start()
+        started += [first, second]
+    metas_ref[level] = meta_ref[level]
+    slots = plane * capacity
+    group_rows = rows_ref.shape[1]
+    locals_ = []
+    for d in level_order(groups):
+        source = lax.rem(level + groups - d, groups)
+        if d == 0:
+            rows, info = rows_ref[level], meta_ref[level]
+        else:
+            peer = (source * plane + place, core)
+            remote(meta_ref.at[source], metas_ref.at[source], m_send.at[d], m_recv.at[source], peer).wait_recv()
+            remote(rows_ref.at[source], landed.at[source], z_send.at[d], z_recv.at[source], peer).wait_recv()
+            rows, info = landed[source], metas_ref[source]
+        info = info[:, :group_rows].astype(jnp.float32)
+        slot = lax.broadcasted_iota(jnp.int32, (slots, group_rows), 0).astype(jnp.float32)
+        chooser = jnp.where((slot == info[0:1]) | (slot == info[1:2]), 1.0, 0.0)
+        picked = jnp.dot(chooser.astype(jnp.bfloat16), rows, preferred_element_type=jnp.float32)
+        for e in range(plane):
+            spread[d, e] = picked[e * capacity : (e + 1) * capacity].astype(jnp.bfloat16)
+        for far in range(plane - 1, 0, -1):
+            to = lax.rem(place + far, plane)
+            copy = remote(
+                spread.at[d, to], out_ref.at[core, source, place],
+                p_send.at[d * plane + far], p_recv.at[source * plane + place],
+                (level * plane + to, core),
+            )
+            copy.start()
+            started.append(copy)
+        keep = pltpu.make_async_copy(
+            spread.at[d, place], out_ref.at[core, source, place], own_sem.at[d]
+        )
+        keep.start()
+        locals_.append(keep)
+    for at, d in enumerate(level_order(groups)):
+        source = lax.rem(level + groups - d, groups)
+        for far in range(1, plane):
+            origin = lax.rem(place + plane - far, plane)
+            remote(
+                spread.at[d, origin], out_ref.at[core, source, origin],
+                p_send.at[d * plane + far], p_recv.at[source * plane + origin],
+                (level * plane + origin, core),
+            ).wait_recv()
+        locals_[at].wait()
+        copy = remote(
+            out_ref.at[core, source], out_ref.at[core, source],
+            t_send.at[d], t_recv.at[source], (index, 1 - core),
+        )
+        copy.start()
+        started.append(copy)
+    for d in level_order(groups):
+        source = lax.rem(level + groups - d, groups)
+        remote(
+            out_ref.at[1 - core, source], out_ref.at[1 - core, source],
+            t_send.at[d], t_recv.at[source], (index, 1 - core),
+        ).wait_recv()
+    for copy in started:
+        copy.wait_send()
+
+
+def return_kernel(
+    groups, plane, capacity, part_ref, metas_ref, out_ref,
+    passed, mixed, back, merged, t_send, t_recv, p_send, p_recv, own_sem, z_send, z_recv,
+):
+    index, core, level, place = greet(groups, plane)
+    started, locals_ = [], []
+    order = level_order(groups)[::-1]
+    slots = plane * capacity
+    group_rows = out_ref.shape[1]
+    for d in order:
+        goal = lax.rem(level + d, groups)
+        copy = remote(
+            part_ref.at[1 - core, goal], passed.at[goal], t_send.at[d], t_recv.at[goal],
+            (index, 1 - core),
+        )
+        copy.start()
+        started.append(copy)
+    for d in order:
+        goal = lax.rem(level + d, groups)
+        remote(
+            part_ref.at[core, goal], passed.at[goal], t_send.at[d], t_recv.at[goal],
+            (index, 1 - core),
+        ).wait_recv()
+        for e in range(plane):
+            mixed[d, e] = (
+                part_ref[core, goal, e].astype(jnp.float32) + passed[goal, e].astype(jnp.float32)
+            ).astype(jnp.bfloat16)
+        for far in range(plane - 1, 0, -1):
+            to = lax.rem(place + far, plane)
+            copy = remote(
+                mixed.at[d, to], back.at[goal, place],
+                p_send.at[d * plane + far], p_recv.at[goal * plane + place],
+                (level * plane + to, core),
+            )
+            copy.start()
+            started.append(copy)
+        keep = pltpu.make_async_copy(mixed.at[d, place], back.at[goal, place], own_sem.at[d])
+        keep.start()
+        locals_.append(keep)
+    for at, d in enumerate(order):
+        goal = lax.rem(level + d, groups)
+        for far in range(1, plane):
+            origin = lax.rem(place + plane - far, plane)
+            remote(
+                mixed.at[d, origin], back.at[goal, origin],
+                p_send.at[d * plane + far], p_recv.at[goal * plane + origin],
+                (level * plane + origin, core),
+            ).wait_recv()
+        locals_[at].wait()
+        info = metas_ref[goal][:, :group_rows].astype(jnp.float32)
+        slot = lax.broadcasted_iota(jnp.int32, (slots, group_rows), 0).astype(jnp.float32)
+        hit_first, hit_second = slot == info[0:1], slot == info[1:2]
+        arrived = back[goal].reshape(slots, back.shape[-1])
+        result = 0.0
+        for term in range(2):
+            share = jnp.where(hit_first, info[2 + term : 3 + term], 0.0) + jnp.where(
+                hit_second, info[4 + term : 5 + term], 0.0
+            )
+            result = result + lax.dot_general(
+                share.astype(jnp.bfloat16), arrived, (((0,), (0,)), ((), ())),
+                preferred_element_type=jnp.float32,
+            )
+        if d == 0:
+            out_ref[level] = result.astype(jnp.bfloat16)
+        else:
+            merged[d] = result.astype(jnp.bfloat16)
+            copy = remote(
+                merged.at[d], out_ref.at[level], z_send.at[d], z_recv.at[level],
+                (goal * plane + place, core),
+            )
+            copy.start()
+            started.append(copy)
+    for d in range(1, groups):
+        other = lax.rem(level + groups - d, groups)
+        remote(
+            merged.at[d], out_ref.at[other], z_send.at[d], z_recv.at[other],
+            (other * plane + place, core),
+        ).wait_recv()
+    for copy in started:
+        copy.wait_send()
+
+
+def dispatch(rows, meta, plane, capacity):
+    groups, group_rows, width = rows.shape
+    vmem = pl.BlockSpec(memory_space=pltpu.VMEM)
+    dma = pltpu.SemaphoreType.DMA
+    few, many = dma((groups,)), dma((groups * plane,))
+    return pl.pallas_call(
+        functools.partial(dispatch_kernel, groups, plane, capacity),
+        out_shape=(
+            jax.ShapeDtypeStruct((2, groups, plane, capacity, width), jnp.bfloat16),
+            jax.ShapeDtypeStruct(meta.shape, jnp.bfloat16),
+        ),
+        in_specs=[vmem, vmem],
+        out_specs=(vmem, vmem),
+        scratch_shapes=[
+            pltpu.VMEM((groups, group_rows, width), jnp.bfloat16),
+            pltpu.VMEM((groups, plane, capacity, width), jnp.bfloat16),
+            few, few, few, few, many, many, few, few, few,
+        ],
+        compiler_params=pltpu.CompilerParams(
+            collective_id=1, has_side_effects=True, vmem_limit_bytes=40 * 1024 * 1024
+        ),
+        name="dispatch",
+    )(rows, meta)
+
+
+def give_back(partial_value, metas, group_rows):
+    _, groups, plane, capacity, width = partial_value.shape
+    vmem = pl.BlockSpec(memory_space=pltpu.VMEM)
+    dma = pltpu.SemaphoreType.DMA
+    few, many = dma((groups,)), dma((groups * plane,))
+    block = pltpu.VMEM((groups, plane, capacity, width), jnp.bfloat16)
+    return pl.pallas_call(
+        functools.partial(return_kernel, groups, plane, capacity),
+        out_shape=jax.ShapeDtypeStruct((groups, group_rows, width), jnp.bfloat16),
+        in_specs=[vmem, vmem],
+        out_specs=vmem,
+        scratch_shapes=[
+            block, block, block,
+            pltpu.VMEM((groups, group_rows, width), jnp.bfloat16),
+            few, few, many, many, few, few, few,
+        ],
+        compiler_params=pltpu.CompilerParams(
+            collective_id=2, has_side_effects=True, vmem_limit_bytes=40 * 1024 * 1024
+        ),
+        name="give_back",
+    )(partial_value, metas)
+
+
 def local(
     residual,
     queries,
@@ -192,35 +424,48 @@
     )
     earlier = jnp.cumsum(onehot, axis=0) - onehot
     slot_rank = jnp.sum(earlier * onehot, axis=1)
-    slot_ids = (flat_ids * capacity + slot_rank).reshape(row_count, top_count)
-    matches = (
-        slot_ids[:, :, None]
-        == jnp.arange(expert_count * capacity, dtype=jnp.int32)[None, None, :]
-    )
-    chooser = jnp.any(matches, axis=1).astype(jnp.bfloat16)
-    buffer = lax.dot_general(
+    plane = expert_count // GROUPS
+    group_rows = capacity * plane // top_count
+    group_of = expert_ids[:, 0] // plane
+    in_group = (group_of[:, None] == jnp.arange(GROUPS, dtype=jnp.int32)[None, :]).astype(jnp.int32)
+    group_rank = jnp.sum((jnp.cumsum(in_group, axis=0) - in_group) * in_group, axis=1)
+    slots = (lax.rem(flat_ids, plane) * capacity + slot_rank).reshape(row_count, top_count)
+    member = (group_of * group_rows + group_rank)[:, None]
+    chooser = (member == jnp.arange(GROUPS * group_rows, dtype=jnp.int32)[None, :]).astype(
+        jnp.bfloat16
+    )
+    coarse = route_weight.astype(jnp.bfloat16)
+    fine = (route_weight - coarse.astype(jnp.float32)).astype(jnp.bfloat16)
+    fields = jnp.concatenate(
+        [
+            (slots + 1).astype(jnp.bfloat16),
+            jnp.stack([coarse[:, 0], fine[:, 0], coarse[:, 1], fine[:, 1]], axis=1),
+        ],
+        axis=1,
+    )
+    fields = jnp.pad(fields, ((0, 0), (0, 16 - fields.shape[1])))
+    meta = lax.dot_general(
+        fields, chooser, (((0,), (0,)), ((), ())), preferred_element_type=jnp.float32
+    )
+    meta = meta - (jnp.arange(16) < top_count)[:, None].astype(jnp.float32)
+    meta = meta.astype(jnp.bfloat16).reshape(16, GROUPS, group_rows).transpose(1, 0, 2)
+    meta = jnp.pad(meta, ((0, 0), (0, 0), (0, -group_rows % 128)))
+    grouped = lax.dot_general(
         chooser, normed, (((0,), (0,)), ((), ())), preferred_element_type=jnp.float32
     ).astype(jnp.bfloat16)
-    buffer = buffer.reshape(expert_count, capacity, width)
-    arrived = lax.all_to_all(buffer, "sp", split_axis=0, concat_axis=0, tiled=True)
-    both_halves = lax.all_gather(arrived, "tp", axis=0, tiled=True)
-    flat_rows = both_halves.reshape(-1, width)
+    arrived, metas = dispatch(
+        grouped.reshape(GROUPS, group_rows, width), meta, plane, capacity
+    )
+    flat_rows = arrived.reshape(-1, width)
     gate_out = jnp.dot(flat_rows, gate_weight[0], preferred_element_type=jnp.float32)
     upward = jnp.dot(flat_rows, up_weight[0], preferred_element_type=jnp.float32)
     hidden = (jax.nn.silu(gate_out) * upward).astype(jnp.bfloat16)
-    partial_value = jnp.dot(hidden, down_weight[0], preferred_element_type=jnp.float32).reshape(
-        both_halves.shape
-    )
-    summed = lax.psum_scatter(
-        partial_value.astype(jnp.bfloat16), "tp", scatter_dimension=0, tiled=True
-    )
-    returned = lax.all_to_all(summed, "sp", split_axis=0, concat_axis=0, tiled=True)
-    share = jnp.sum(jnp.where(matches, route_weight[:, :, None], 0.0), axis=1)
-    coarse = share.astype(jnp.bfloat16)
-    fine = (share - coarse.astype(jnp.float32)).astype(jnp.bfloat16)
-    flat = returned.reshape(-1, width)
-    expert_mix = jnp.dot(coarse, flat, preferred_element_type=jnp.float32) + jnp.dot(
-        fine, flat, preferred_element_type=jnp.float32
+    partial_value = jnp.dot(hidden, down_weight[0], preferred_element_type=jnp.float32)
+    returned = give_back(
+        partial_value.astype(jnp.bfloat16).reshape(arrived.shape), metas, group_rows
+    )
+    expert_mix = jnp.dot(
+        chooser, returned.reshape(-1, width), preferred_element_type=jnp.float32
     )
     return (middle.astype(jnp.float32) + expert_mix).astype(jnp.bfloat16)
 

time: 279 us -> 232 us (0.83); the launches traced: 274 us -> 232 us
  Pallas kernels: 3.31 us -> 102 us
  blocking collectives: 74.1 us -> 3.89 us
  waiting for transfers between devices: 116 us -> 54.6 us
  starting transfers between devices: 7.24 us -> 0.01 us
    pallas_call x0 -> x2, Pallas kernels: none -> 98.6 us  [the longest x1 54 us: dispatch(): pl.pallas_call(functools.partial(dispatch_kernel, groups, plane, capacity...]
    all_to_all x1 -> x0, blocking collectives: 70.2 us -> none  [local(): lax.all_to_all(buffer, 'sp', split_axis=0, concat_axis=0, tiled=True)]
    all_to_all x1 -> x0, waiting for transfers between devices: 43.2 us -> none  [local(): lax.all_to_all(summed, 'sp', split_axis=0, concat_axis=0, tiled=True)]
    reduce_scatter x1 -> x0, waiting for transfers between devices: 13.3 us -> none  [local(): lax.psum_scatter(partial_value.astype(jnp.bfloat16), 'tp', scatter_dimens...]
    all_gather x1 -> x0, waiting for transfers between devices: 11.9 us -> none  [local(): both_halves = lax.all_gather(arrived, 'tp', axis=0, tiled=True)]
    all_gather x1, waiting for transfers between devices: 47.1 us -> 54.6 us  [local(): packed = lax.all_gather(own, 'sp', axis=0, tiled=True)]
    all_to_all x1 -> x0, starting transfers between devices: 6.98 us -> none  [local(): lax.all_to_all(summed, 'sp', split_axis=0, concat_axis=0, tiled=True)]
    dot_general x1, matrix products: 4.27 us -> 10.7 us  [local(): jnp.dot(hidden, down_weight[0], preferred_element_type=jnp.float32)]
  transfers between devices with their start and end apart: 4 -> 1, of which waited for: 4 -> 1; matrix products, arithmetic and copies ran while one was open for 8% -> 6% of each run, Pallas kernels for 0% -> 0%
where the time goes in v2:
time: 232 us
  Pallas kernels  102 us (44%)
  waiting for transfers between devices  54.6 us (24%)
  local copies, waits for them, and re-layouts  23.9 us (10%)
  between operations  19 us (8%)
  matrix products  17 us (7%)
  other arithmetic  11.6 us (5%)
  blocking collectives  3.89 us (2%)
    all_gather x1, waiting for transfers between devices, local(): packed = lax.all_gather(own, 'sp', axis=0, tiled=True)  54.6 us
    pallas_call x1, Pallas kernels, dispatch(): pl.pallas_call(functools.partial(dispatch_kernel, groups, plane, capacity...  54 us
    pallas_call x1, Pallas kernels, give_back(): pl.pallas_call(functools.partial(return_kernel, groups, plane, capacity),...  44.6 us
    unnamed x39, local copies, waits for them, and re-layouts  13.6 us
    dot_general x1, matrix products, local(): jnp.dot(hidden, down_weight[0], preferred_element_type=jnp.float32)  10.7 us
  transfers between devices with their start and end apart: 1, of which 1 were waited for; matrix products, arithmetic and copies ran while one was open for 6% of the time, Pallas kernels for 0%

profile of v2, /device:TPU:0, one launch (start us, length us, event | category | flops | bytes accessed | tf_op | source)
XLA Modules:
  0.0 231.9 jit_solution(3343898828100070368)
XLA Ops:
  6.5 0.0 copy-start
  6.6 0.5 multiply_power_fusion
  7.1 0.7 convert_element_type.91
  7.8 0.7 slice_convert_fusion
  8.5 0.1 broadcast_in_dim.15
  8.6 0.1 copy.74
  8.7 0.1 copy.73
  8.8 2.0 fusion.20
  10.8 1.8 concatenate.12
  12.6 0.0 all-gather.2.cloned.1.call-update
  12.6 0.6 slice.40
  14.5 0.8 copy.81
  15.3 0.1 eq.67
  15.4 0.1 eq.63
  16.9 0.6 reduce-window.6
  17.5 0.2 slice_reduce_fusion
  17.7 0.1 fusion.27
  17.8 0.1 reduce_sum.55
  18.0 0.1 copy.84
  18.1 0.1 fusion.24
  18.2 0.2 reduce_window_sum.26
  18.3 0.0 copy-done.16
  18.4 0.2 select_reduce_fusion
  18.6 0.2 fusion.8
  18.8 0.1 reshape.92
  18.9 0.2 copy-done.14
  19.1 1.1 copy.77
  20.2 0.8 pad.12
  21.0 1.2 copy.79.wk_ref
  22.1 1.9 copy.78.query_ref
  24.0 0.7 broadcast_in_dim.13
  24.7 0.7 mul.104
  25.3 0.7 broadcast_in_dim.14
  26.0 2.3 concatenate.13.table_ref
  28.2 0.6 iota_add_fusion
  28.8 54.6 %all-gather.2.cloned.1.call-done.packed_ref = bf16[4096,384]{1,0:T(8,128)(2,1)} async-done(((bf16[256,384]{1,0:T(8,128)(2,1)}), bf16[4096,384]{1,0:T(8,128)(2,1)}) %all-gather.2.cloned.1.call-update) | async-done | bytes 3145744 | tf_op jit(solution)/shard_map/all_gather | solution.py:407
  83.4 2.1 convert_reduce_fusion.1
  85.5 2.6 %convert_reduce_fusion = s32[256]{0:T(256)S(1)} fusion(s32[256]{0:T(256)} %param.19, s32[4096]{0:T(1024)S(1)} %convert_reduce_fusion.1), kind=kLoop, calls=%fused_computation | loop fusion | flops 3145472 | bytes 18432 | tf_op jit(solution)/shard_map/reduce_sum | solution.py:111
  88.1 0.5 copy-done.13
  88.6 0.6 slice.39
  91.9 0.1 pad_add_fusion.1.lo_ref
  92.0 0.7 pad_add_fusion.span_ref
  92.7 1.9 copy-done.1
  94.6 1.0 copy-done.3
  95.5 0.9 copy-done.4
  96.5 0.9 copy-done.5
  97.4 3.3 %attend.1 = bf16[384,256]{1,0:T(8,128)(2,1)S(1)} custom-call(s32[2]{0:T(128)S(1)} %pad_add_fusion.1.lo_ref, bf16[256,576]{1,0:T(8,128)(2,1)S(1)} %copy-done.3, f32[256,256]{1,0:T(8,128)S(1)} %copy-done.4, s32[2,256]{1,0:T(2,128)S(1)} %pad_add_fusion.span_ref, bf16[4096,384]{1,0:T(8,128)(2,1)S(1)} %copy-done.1, bf16[256,768]{1,0:T(8,128)(2,1)S(1)} %copy.79.wk_ref, ...), custom_call_target="tpu_custom_call" | custom-call | tf_op jit(solution)/shard_map/attend/pallas_call | solution.py:124
  100.8 3.9 %all_to_all.19 = bf16[2,128,384]{1,2,0:T(8,128)(2,1)S(1)} all-to-all(bf16[2,128,384]{1,2,0:T(8,128)(2,1)S(1)} %copy_bitcast_fusion), channel_id=1, replica_groups=mesh['sp'=16,'tp'=2] {'tp'}, dimensions={0} | all-to-all | bytes 393216 | tf_op jit(solution)/shard_map/all_to_all | solution.py:411
  104.7 0.0 copy-done
  104.7 0.7 multiply_reduce_fusion
  105.4 0.3 copy-done.9
  105.7 0.2 add_convert_fusion
  105.9 0.0 copy-start.7
  105.9 0.0 copy-start.17
  106.0 0.2 fusion.9
  106.2 0.5 convolution_convert_fusion.1
  106.7 0.0 copy-done.7
  106.7 54.0 %dispatch.1 = (bf16[2,4,4,32,2048]{4,3,2,1,0:T(8,128)(2,1)S(1)}, bf16[4,16,128]{2,1,0:T(8,128)(2,1)S(1)}) custom-call(bf16[4,64,2048]{2,1,0:T(8,128)(2,1)S(1)} %bitcast.70, bf16[4,16,128]{2,1,0:T(8,128)(2,1)S(1)} %pad.14.meta_ref), custom_call_target="tpu_custom_call" | custom-call | tf_op jit(solution)/shard_map/dispatch/pallas_call | solution.py:329
  160.7 1.9 copy-done.6
  162.6 3.7 %fusion.2 = f32[1024,512]{1,0:T(8,128)} fusion(bf16[1024,2048]{1,0:T(8,128)(2,1)S(1)} %bitcast.71, bf16[1,2048,512]{2,1,0:T(8,128)(2,1)S(1)} %copy-done.17), kind=kOutput, calls=%fused_computation.6 | convolution fusion | flops 2147483648 | bytes 8388608 | tf_op jit(solution)/shard_map/dot_general | solution.py:461
  166.4 10.7 %convolution_convert_fusion = bf16[1024,2048]{1,0:T(8,128)(2,1)} fusion(bf16[1,512,2048]{2,1,0:T(8,128)(2,1)} %param.29, f32[1024,512]{1,0:T(8,128)} %fusion.2, bf16[1024,2048]{1,0:T(8,128)(2,1)} %bitcast.72, bf16[1,2048,512]{2,1,0:T(8,128)(2,1)} %param.27), kind=kOutput, calls=%fused_computation.1 | convolution fusion | flops 4300210176 | bytes 14680064 | tf_op jit(solution)/shard_map/dot_general | solution.py:463
  177.1 2.2 copy-done.2
  179.3 44.6 %give_back.1 = bf16[4,64,2048]{2,1,0:T(8,128)(2,1)S(1)} custom-call(bf16[2,4,4,32,2048]{4,3,2,1,0:T(8,128)(2,1)S(1)} %bitcast.69, bf16[4,16,128]{2,1,0:T(8,128)(2,1)S(1)} %get-tuple-element.8.metas_ref), custom_call_target="tpu_custom_call" | custom-call | tf_op jit(solution)/shard_map/give_back/pallas_call | solution.py:355
  223.9 1.1 fusion
  (40 shorter events, 0.2 us)
Async XLA Ops:
  6.5 98.1 %copy-start = (bf16[768,2048]{1,0:T(8,128)(2,1)S(1)}, bf16[768,2048]{1,0:T(8,128)(2,1)}, u32[]{:S(2)}) copy-start(bf16[768,2048]{1,0:T(8,128)(2,1)} %param.22) | copy-start | bytes 9437188
  6.5 11.5 %copy-start.12 = (s32[128,2]{0,1:T(2,128)S(1)}, s32[128,2]{0,1:T(2,128)}, u32[]{:S(2)}) copy-start(s32[128,2]{0,1:T(2,128)} %param.25) | copy-start | bytes 3076
  6.5 11.8 %copy-start.16 = (f32[128,2]{0,1:T(2,128)S(1)}, f32[128,2]{0,1:T(2,128)}, u32[]{:S(2)}) copy-start(f32[128,2]{0,1:T(2,128)} %param.26) | copy-start | bytes 3076
  6.5 76.8 %all-gather.2.cloned.1.call-start = ((), (), s32[]{:S(2)}) async-start(), calls=%async_computation.1 | async-start | bytes 3342336 | tf_op jit(solution)/shard_map/all_gather | solution.py:407
  18.6 0.5 copy-start.14
  88.1 0.5 copy-start.13
  92.7 1.9 copy-start.1
  94.6 1.0 copy-start.3
  95.5 0.9 copy-start.4
  96.5 0.9 copy-start.5
  104.7 1.0 copy-start.9
  104.7 1.0 copy-start.10
  105.3 0.8 copy-start.11
  105.4 0.8 copy-start.15
  105.9 0.8 copy-start.7
  105.9 56.7 %copy-start.17 = (bf16[1,2048,512]{2,1,0:T(8,128)(2,1)S(1)}, bf16[1,2048,512]{2,1,0:T(8,128)(2,1)}, u32[]{:S(2)}) copy-start(bf16[1,2048,512]{2,1,0:T(8,128)(2,1)} %param.28) | copy-start | bytes 6291460
  160.7 1.9 copy-start.6
  177.1 2.2 copy-start.2
  179.3 44.6 %copy-start.8 = (bf16[128,2048]{1,0:T(8,128)(2,1)S(1)}, bf16[128,2048]{1,0:T(8,128)(2,1)}, u32[]{:S(2)}) copy-start(bf16[128,2048]{1,0:T(8,128)(2,1)} %copy-done.7) | copy-start | bytes 1572868
Sparse Core Ops, SparseCore 0:
  12.7 70.5 all-gather.1

commit v3 on v2

--- a/solution.py
+++ b/solution.py
@@ -22,6 +22,9 @@
 def angles_of(positions):
     half_width = ROPE // 2
     frequency = rope_base ** (-jnp.arange(half_width, dtype=jnp.float32) / half_width)
+    lane = jnp.arange(HEAD_LANES)
+    turns = (lane >= UNROTATED_DIM) & (lane < UNROTATED_DIM + ROPE)
+    frequency = jnp.where(turns, jnp.tile(frequency, HEAD_LANES // half_width), 0.0)
     angles = positions.astype(jnp.float32)[:, None] * frequency[None, :]
     return jnp.cos(angles), jnp.sin(angles)
 
@@ -31,15 +34,15 @@
 
 
 def attention_kernel(
-    heads, block, lo_ref, query_ref, table_ref, span_ref, packed_ref, wk_ref, wv_ref, out_ref,
-    turned, high, total, acc,
+    heads, block, lo_ref, query_ref, cos_ref, sin_ref, span_ref, packed_ref, wk_ref, wv_ref, out_ref,
+    turned, wide, high, total, acc,
 ):
     rows = query_ref.shape[0]
     width = query_ref.shape[1]
     rank = wk_ref.shape[0]
     per_head = UNROTATED_DIM + ROPE
-    cosine = table_ref[:, :HEAD_LANES]
-    sine = table_ref[:, HEAD_LANES:]
+    cosine = cos_ref[...]
+    sine = sin_ref[...]
     for h in range(heads):
         first = h * per_head // 128 * 128
         last = min(-(-(h + 1) * per_head // 128) * 128, width)
@@ -54,6 +57,12 @@
         crossed = (jnp.where(lower, 1.0, 0.0) - jnp.where(upper, 1.0, 0.0)).astype(jnp.bfloat16)
         straight = jnp.dot(window, plain, preferred_element_type=jnp.float32)
         swapped = jnp.dot(window, crossed, preferred_element_type=jnp.float32)
+        low = h * UNROTATED_DIM // HEAD_LANES * HEAD_LANES
+        pair = wk_ref[:, low : low + HEAD_LANES].astype(jnp.float32)
+        if h * UNROTATED_DIM > low:
+            pair = pltpu.roll(pair, HEAD_LANES - (h * UNROTATED_DIM - low), 1)
+        column = lax.broadcasted_iota(jnp.int32, pair.shape, 1)
+        wide[h] = jnp.where(column < UNROTATED_DIM, pair, 0.0).astype(jnp.bfloat16)
         turned[h] = (straight * cosine + swapped * sine).astype(jnp.bfloat16)
     high[...] = jnp.full(high.shape, -1e30, jnp.float32)
     total[...] = jnp.zeros(total.shape, jnp.float32)
@@ -73,7 +82,7 @@
         ).astype(jnp.bfloat16)
         for h in range(heads):
             keys = jnp.dot(
-                latent, wk_ref[:, h * HEAD_LANES : (h + 1) * HEAD_LANES],
+                latent, wide[h],
                 preferred_element_type=jnp.float32,
             ).astype(jnp.bfloat16) + extra
             scores = lax.dot_general(
@@ -107,34 +116,30 @@
     heads = queries.shape[1] // (UNROTATED_DIM + ROPE)
     rank = latent_to_key.shape[0]
     count = packed.shape[0]
+    place = jnp.arange(count, dtype=jnp.int32)
     docs = packed[:, rank + UNROTATED_DIM + ROPE].astype(jnp.int32)
+    docs = jnp.where(place < positions[0] - count // 2, -1, docs)
+    docs = jnp.where(place > positions[-1], jnp.iinfo(jnp.int32).max, docs)
     starts = jnp.sum((docs[:, None] < doc_ids[None, :]).astype(jnp.int32), axis=0)
     block = math.gcd(count, 256)
     bounds = jnp.stack([starts[0] // block, positions[-1] // block + 1]).astype(jnp.int32)
     span = jnp.stack([starts, positions])
-    one, none = jnp.ones((rows, UNROTATED_DIM)), jnp.zeros((rows, HEAD_LANES - UNROTATED_DIM - ROPE))
-    table = jnp.concatenate(
-        [one, cosine, cosine, none, 0.0 * one, sine, sine, none], axis=1
-    ).astype(jnp.float32)
-    wk = jnp.pad(
-        latent_to_key.reshape(rank, heads, UNROTATED_DIM),
-        ((0, 0), (0, 0), (0, HEAD_LANES - UNROTATED_DIM)),
-    ).reshape(rank, heads * HEAD_LANES)
     vmem = pl.BlockSpec(memory_space=pltpu.VMEM)
     out = pl.pallas_call(
         functools.partial(attention_kernel, heads, block),
         out_shape=jax.ShapeDtypeStruct((heads * VALUE_ENTRIES, rows), jnp.bfloat16),
-        in_specs=[pl.BlockSpec(memory_space=pltpu.SMEM)] + [vmem] * 6,
+        in_specs=[pl.BlockSpec(memory_space=pltpu.SMEM)] + [vmem] * 7,
         out_specs=vmem,
         scratch_shapes=[
             pltpu.VMEM((heads, rows, HEAD_LANES), jnp.bfloat16),
+            pltpu.VMEM((heads, rank, HEAD_LANES), jnp.bfloat16),
             pltpu.VMEM((heads, rows), jnp.float32),
             pltpu.VMEM((heads, rows), jnp.float32),
             pltpu.VMEM((heads, VALUE_ENTRIES, rows), jnp.float32),
         ],
         compiler_params=pltpu.CompilerParams(vmem_limit_bytes=40 * 1024 * 1024),
         name="attend",
-    )(bounds, queries, table, span, packed, wk, latent_to_value)
+    )(bounds, queries, cosine, sine, span, packed, latent_to_key, latent_to_value)
     return out.T
 
 
@@ -369,6 +374,118 @@
     )(partial_value, metas)
 
 
+def spread_kernel(
+    groups, plane, own_ref, out_ref, z_send, z_recv, p_send, p_recv, t_send, t_recv
+):
+    index, core, level, place = greet(groups, plane)
+    reach = groups // 2
+    rows = own_ref.shape[0]
+    half = rows // 2
+    mine = pl.ds(pl.multiple_of(core * half, half), half)
+    other = pl.ds(pl.multiple_of((1 - core) * half, half), half)
+
+    def z_copy(d):
+        return remote(
+            own_ref.at[mine], out_ref.at[index, mine], z_send.at[d], z_recv.at[d],
+            (lax.rem(level + d, groups) * plane + place, core),
+        )
+
+    def z_arrival(d):
+        block = lax.rem(level + groups - d, groups) * plane + place
+        return remote(
+            own_ref.at[mine], out_ref.at[block, mine], z_send.at[d], z_recv.at[d],
+            (block, core),
+        )
+
+    def p_copy(d, far):
+        block = lax.rem(level + groups - d, groups) * plane + place
+        source = own_ref.at[mine] if d == 0 else out_ref.at[block, mine]
+        return remote(
+            source, out_ref.at[block, mine], p_send.at[d * plane + far],
+            p_recv.at[d * plane + far],
+            (level * plane + lax.rem(place + far, plane), core),
+        )
+
+    def p_arrival(d, far):
+        origin = lax.rem(place + plane - far, plane)
+        block = lax.rem(level + groups - d, groups) * plane + origin
+        return remote(
+            own_ref.at[mine], out_ref.at[block, mine], p_send.at[d * plane + far],
+            p_recv.at[d * plane + far], (level * plane + origin, core),
+        )
+
+    def t_copy(d, far, part):
+        origin = lax.rem(place + plane - far, plane)
+        block = lax.rem(level + groups - d, groups) * plane + origin
+        return remote(
+            out_ref.at[block, part], out_ref.at[block, part], t_send.at[d * plane + far],
+            t_recv.at[d * plane + far], (index, 1 - core),
+        )
+
+    def wanted(d, far, sender):
+        ahead = lax.rem(place + far, plane) > place if sender else place >= far
+        live = level >= d
+        if d == 0:
+            return live & ahead
+        if d == reach:
+            return live & jnp.logical_not(ahead)
+        return live
+
+    for d in range(reach, 0, -1):
+        pl.when(level + d < groups)(lambda d=d: z_copy(d).start())
+    for far in range(1, plane):
+        pl.when(wanted(0, far, True))(lambda far=far: p_copy(0, far).start())
+    out_ref[index] = own_ref[...]
+    for d in range(1, reach + 1):
+
+        def arrived(d=d):
+            z_arrival(d).wait_recv()
+            t_copy(d, 0, mine).start()
+
+        pl.when(level >= d)(arrived)
+        for far in range(1, plane):
+            pl.when(wanted(d, far, True))(lambda d=d, far=far: p_copy(d, far).start())
+    for d in range(reach + 1):
+        for far in range(1, plane):
+
+            def passed_on(d=d, far=far):
+                p_arrival(d, far).wait_recv()
+                t_copy(d, far, mine).start()
+
+            pl.when(wanted(d, far, False))(passed_on)
+    for d in range(reach + 1):
+        for far in range(0 if d else 1, plane):
+
+            def from_partner(d=d, far=far):
+                t_copy(d, far, other).wait_recv()
+                t_copy(d, far, mine).wait_send()
+
+            pl.when((level >= d) if far == 0 else wanted(d, far, False))(from_partner)
+            if far:
+                pl.when(wanted(d, far, True))(lambda d=d, far=far: p_copy(d, far).wait_send())
+    for d in range(1, reach + 1):
+        pl.when(level + d < groups)(lambda d=d: z_copy(d).wait_send())
+
+
+def spread_blocks(own, count):
+    rows, lanes = own.shape
+    plane = count // GROUPS
+    vmem = pl.BlockSpec(memory_space=pltpu.VMEM)
+    few = pltpu.SemaphoreType.DMA((GROUPS,))
+    many = pltpu.SemaphoreType.DMA((GROUPS * plane,))
+    return pl.pallas_call(
+        functools.partial(spread_kernel, GROUPS, plane),
+        out_shape=jax.ShapeDtypeStruct((count, rows, lanes), jnp.bfloat16),
+        in_specs=[vmem],
+        out_specs=vmem,
+        scratch_shapes=[few, few, many, many, many, many],
+        compiler_params=pltpu.CompilerParams(
+            collective_id=3, has_side_effects=True, vmem_limit_bytes=40 * 1024 * 1024
+        ),
+        name="spread_blocks",
+    )(own).reshape(count * rows, lanes)
+
+
 def local(
     residual,
     queries,
@@ -390,21 +507,17 @@
     positions = lax.axis_index("sp") * local_rows + jnp.arange(local_rows, dtype=jnp.int32)
     cosine, sine = angles_of(positions)
     half = ROPE // 2
-    upper, lower = rope_key[:, :half].astype(jnp.float32), rope_key[:, half:].astype(jnp.float32)
-    key_rot = jnp.concatenate(
-        [upper * cosine - lower * sine, lower * cosine + upper * sine], axis=1
+    after = HEAD_LANES - UNROTATED_DIM - ROPE
+    key = rope_key.astype(jnp.float32)
+    crossed = jnp.concatenate([-key[:, half:], key[:, :half]], axis=1)
+    around = ((0, 0), (UNROTATED_DIM, after))
+    extra = jnp.pad(key, around) * cosine + jnp.pad(crossed, around) * sine
+    lane = jnp.arange(HEAD_LANES)[None, :]
+    extra = jnp.where(
+        lane == UNROTATED_DIM + ROPE, doc_ids.astype(jnp.float32)[:, None], extra
     ).astype(jnp.bfloat16)
-    own = jnp.concatenate(
-        [
-            latent,
-            jnp.zeros((local_rows, UNROTATED_DIM), jnp.bfloat16),
-            key_rot,
-            doc_ids.astype(jnp.bfloat16)[:, None],
-            jnp.zeros((local_rows, HEAD_LANES - UNROTATED_DIM - ROPE - 1), jnp.bfloat16),
-        ],
-        axis=1,
-    )
-    packed = lax.all_gather(own, "sp", axis=0, tiled=True)
+    own = jnp.concatenate([latent, extra], axis=1)
+    packed = spread_blocks(own, lax.axis_size("sp"))
     attended = attend(
         queries, packed, doc_ids, latent_to_key, latent_to_value, positions, cosine, sine
     )
@@ -418,18 +531,19 @@
     top_count = expert_ids.shape[1]
     expert_count = lax.axis_size("sp")
     capacity = row_count // (expert_count // GROUPS)
-    flat_ids = expert_ids.reshape(-1)
-    onehot = (flat_ids[:, None] == jnp.arange(expert_count, dtype=jnp.int32)[None, :]).astype(
-        jnp.int32
-    )
-    earlier = jnp.cumsum(onehot, axis=0) - onehot
-    slot_rank = jnp.sum(earlier * onehot, axis=1)
     plane = expert_count // GROUPS
     group_rows = capacity * plane // top_count
     group_of = expert_ids[:, 0] // plane
-    in_group = (group_of[:, None] == jnp.arange(GROUPS, dtype=jnp.int32)[None, :]).astype(jnp.int32)
-    group_rank = jnp.sum((jnp.cumsum(in_group, axis=0) - in_group) * in_group, axis=1)
-    slots = (lax.rem(flat_ids, plane) * capacity + slot_rank).reshape(row_count, top_count)
+    bins = jnp.arange(expert_count + GROUPS, dtype=jnp.int32)[None, :]
+    group_bin = group_of[:, None] + expert_count
+    named = jnp.any(expert_ids[:, :, None] == bins[None], axis=1) | (group_bin == bins)
+    before = jnp.arange(row_count)[:, None] > jnp.arange(row_count)[None, :]
+    earlier = jnp.dot(
+        before.astype(jnp.bfloat16), named.astype(jnp.bfloat16), preferred_element_type=jnp.float32
+    ).astype(jnp.int32)
+    slot_rank = jnp.sum(jnp.where(expert_ids[:, :, None] == bins[None], earlier[:, None], 0), axis=2)
+    group_rank = jnp.sum(jnp.where(group_bin == bins, earlier, 0), axis=1)
+    slots = lax.rem(expert_ids, plane) * capacity + slot_rank
     member = (group_of * group_rows + group_rank)[:, None]
     chooser = (member == jnp.arange(GROUPS * group_rows, dtype=jnp.int32)[None, :]).astype(
         jnp.bfloat16

time: 232 us -> 174 us (0.75)
  waiting for transfers between devices: 54.6 us -> 0.62 us
  Pallas kernels: 102 us -> 120 us
  between operations: 19 us -> 6.79 us
  local copies, waits for them, and re-layouts: 23.9 us -> 15.9 us
  blocking collectives: 3.89 us -> 0 us
  other arithmetic: 11.6 us -> 7.8 us
  starting transfers between devices: 0.01 us -> 3.61 us
    all_gather x1 -> x0, waiting for transfers between devices: 54.6 us -> none  [local(): packed = lax.all_gather(own, 'sp', axis=0, tiled=True)]
    pallas_call x0 -> x1, Pallas kernels: none -> 9.96 us  [spread_blocks(): pl.pallas_call(functools.partial(spread_kernel, GROUPS, plane), out_shape...]
    pallas_call x1, Pallas kernels: 54 us -> 60.4 us  [dispatch(): pl.pallas_call(functools.partial(dispatch_kernel, groups, plane, capacity...]
    concatenate x2 -> x0, local copies, waits for them, and re-layouts: 4.03 us -> none  [the longest x1 2.27 us: attend(): jnp.concatenate([one, cosine, cosine, none, 0.0 * one, sine, sine, none],...]
    all_to_all x1 -> x0, blocking collectives: 3.89 us -> none  [local(): lax.all_to_all(attended, 'tp', split_axis=0, concat_axis=1, tiled=True)]
    all_to_all x0 -> x1, starting transfers between devices: none -> 3.61 us  [local(): lax.all_to_all(attended, 'tp', split_axis=0, concat_axis=1, tiled=True)]
    another operation x4 -> x0, other arithmetic: 2.76 us -> none
    unnamed x39 -> x38, local copies, waits for them, and re-layouts: 13.6 us -> 13.7 us
  transfers between devices with their start and end apart: 1 -> 1, of which waited for: 1 -> 1; matrix products, arithmetic and copies ran while one was open for 6% -> 0% of each run, Pallas kernels for 0% -> 0%
where the time goes in v3:
time: 174 us; the launch traced here: 172 us
  Pallas kernels  120 us (69%)
  matrix products  17.2 us (10%)
  local copies, waits for them, and re-layouts  15.9 us (9%)
  other arithmetic  7.8 us (4%)
  between operations  6.79 us (4%)
  starting transfers between devices  3.61 us (2%)
    pallas_call x1, Pallas kernels, dispatch(): pl.pallas_call(functools.partial(dispatch_kernel, groups, plane, capacity...  60.4 us
    pallas_call x1, Pallas kernels, give_back(): pl.pallas_call(functools.partial(return_kernel, groups, plane, capacity),...  46.3 us
    unnamed x38, local copies, waits for them, and re-layouts  13.7 us
    dot_general x1, matrix products, local(): jnp.dot(hidden, down_weight[0], preferred_element_type=jnp.float32)  10.7 us
    pallas_call x1, Pallas kernels, spread_blocks(): pl.pallas_call(functools.partial(spread_kernel, GROUPS, plane), out_shape...  9.96 us
    dot_general x1, matrix products, local(): jnp.dot(flat_rows, up_weight[0], preferred_element_type=jnp.float32)  3.71 us
    all_to_all x1, starting transfers between devices, local(): lax.all_to_all(attended, 'tp', split_axis=0, concat_axis=1, tiled=True)  3.61 us
  transfers between devices with their start and end apart: 1, of which 1 were waited for; matrix products, arithmetic and copies ran while one was open for 0% of the time, Pallas kernels for 0%

profile of v3, /device:TPU:0, one launch (start us, length us, event | category | flops | bytes accessed | tf_op | source)
XLA Modules:
  0.0 171.8 jit_solution(18297619141454089064)
XLA Ops:
  0.0 0.0 copy-start
  0.0 0.7 fusion.37
  2.3 0.8 copy.35
  3.2 0.7 convert_element_type.85
  4.6 0.1 tile.10
  4.7 0.1 slice_negate_fusion
  4.8 1.2 multiply_sine_fusion
  6.0 0.6 fusion.20
  6.6 0.9 pad_maximum_fusion.own_ref
  7.6 0.0 copy-start.15
  7.6 10.0 %spread_blocks.1 = bf16[16,256,384]{2,1,0:T(8,128)(2,1)S(1)} custom-call(bf16[256,384]{1,0:T(8,128)(2,1)S(1)} %pad_maximum_fusion.own_ref), custom_call_target="tpu_custom_call" | custom-call | tf_op jit(solution)/shard_map/spread_blocks/pallas_call | solution.py:476
  18.2 1.7 %select_reduce_fusion = s32[4096]{0:T(1024)S(1)} fusion(bf16[4096,384]{1,0:T(8,128)(2,1)S(1)} %bitcast.49, s32[]{:T(128)} %bitcast.1, s32[]{:T(128)} %bitcast), kind=kLoop, calls=%fused_computation.11 | loop fusion | flops 20480 | bytes 24584 | tf_op jit(solution)/shard_map/jit(_where)/select_n | solution.py:122
  20.0 0.0 copy-start.1
  20.0 1.6 copy-done.1
  21.6 0.0 copy-done.15
  21.6 1.8 %convert_reduce_fusion = s32[256]{0:T(256)S(1)} fusion(s32[256]{0:T(256)S(1)} %copy-done.15, s32[4096]{0:T(1024)S(1)} %select_reduce_fusion), kind=kLoop, calls=%fused_computation | loop fusion | flops 3145472 | bytes 18432 | tf_op jit(solution)/shard_map/reduce_sum | solution.py:123
  23.5 0.6 slice.39
  27.5 1.2 copy.36.query_ref
  28.7 0.1 pad_add_fusion.1.lo_ref
  28.8 0.0 copy-start.2
  28.8 1.9 %copy-done.2 = bf16[16,256,384]{2,1,0:T(8,128)(2,1)S(1)} copy-done((bf16[16,256,384]{2,1,0:T(8,128)(2,1)S(1)}, bf16[16,256,384]{2,1,0:T(8,128)(2,1)}, u32[]{:S(2)}) %copy-start.2) | copy-done | bytes 3145752
  30.7 0.0 copy-start.4
  30.7 0.9 copy-done.4
  31.6 0.0 copy-start.5
  31.6 0.9 copy-done.5
  32.5 0.0 copy-start.6
  32.5 0.9 copy-done.6
  33.4 0.0 copy-start.7
  33.4 0.9 copy-done.7
  34.4 0.0 copy-start.16
  34.4 3.3 %attend.1 = bf16[384,256]{1,0:T(8,128)(2,1)S(1)} custom-call(s32[2]{0:T(128)S(1)} %pad_add_fusion.1.lo_ref, bf16[256,576]{1,0:T(8,128)(2,1)S(1)} %copy.36.query_ref, f32[256,128]{1,0:T(8,128)S(1)} %copy-done.5, f32[256,128]{1,0:T(8,128)S(1)} %copy-done.4, s32[2,256]{1,0:T(2,128)S(1)} %pad_add_fusion.span_ref, bf16[4096,384]{1,0:T(8,128)(2,1)S(1)} %bitcast.50, ...), custom_call_target="tpu_custom_call" | custom-call | tf_op jit(solution)/shard_map/attend/pallas_call | solution.py:128
  37.7 0.7 copy_bitcast_fusion
  38.4 3.6 %all-to-all-start = ((bf16[2,128,384]{1,2,0:T(8,128)(2,1)}), bf16[2,128,384]{1,2,0:T(8,128)(2,1)S(1)}, u32[]{:S(2)}, u32[]{:S(2)}) async-start(bf16[2,128,384]{1,2,0:T(8,128)(2,1)} %copy_bitcast_fusion), calls=%async_computation | async-start | bytes 393216 | tf_op jit(solution)/shard_map/all_to_all | solution.py:524
  42.0 0.0 copy-done.12
  42.1 0.0 copy-done.16
  42.1 0.2 select_reduce_fusion.2
  42.4 0.2 fusion.8
  42.6 0.1 reshape.103
  42.7 0.6 all-to-all-done
  43.3 0.0 copy-done
  43.3 0.0 copy-start.11
  43.3 0.0 copy-start.13
  43.3 0.7 multiply_reduce_fusion
  44.0 0.0 copy-start.14
  44.0 0.3 copy-done.11
  44.4 0.0 copy-done.13
  44.4 0.2 add_convert_fusion
  44.6 0.0 copy-start.9
  44.6 0.0 copy-start.17
  44.6 0.2 fusion.9
  44.8 0.0 copy-done.14
  44.8 0.6 convolution_convert_fusion.1
  45.4 0.0 copy-done.9
  45.4 60.4 %dispatch.1 = (bf16[2,4,4,32,2048]{4,3,2,1,0:T(8,128)(2,1)S(1)}, bf16[4,16,128]{2,1,0:T(8,128)(2,1)S(1)}) custom-call(bf16[4,64,2048]{2,1,0:T(8,128)(2,1)S(1)} %bitcast.53, bf16[4,16,128]{2,1,0:T(8,128)(2,1)S(1)} %pad.18.meta_ref), custom_call_target="tpu_custom_call" | custom-call | tf_op jit(solution)/shard_map/dispatch/pallas_call | solution.py:334
  105.8 0.0 copy-start.8
  105.8 1.9 %copy-done.8 = bf16[2,4,4,32,2048]{4,3,2,1,0:T(8,128)(2,1)} copy-done((bf16[2,4,4,32,2048]{4,3,2,1,0:T(8,128)(2,1)}, bf16[2,4,4,32,2048]{4,3,2,1,0:T(8,128)(2,1)S(1)}, u32[]{:S(2)}) %copy-start.8) | copy-done | bytes 4194328
  107.7 0.0 copy-done.17
  107.7 3.7 %fusion.2 = f32[1024,512]{1,0:T(8,128)} fusion(bf16[1024,2048]{1,0:T(8,128)(2,1)S(1)} %bitcast.54, bf16[1,2048,512]{2,1,0:T(8,128)(2,1)S(1)} %copy-done.17), kind=kOutput, calls=%fused_computation.6 | convolution fusion | flops 2147483648 | bytes 8388608 | tf_op jit(solution)/shard_map/dot_general | solution.py:575
  111.4 10.7 %convolution_convert_fusion = bf16[1024,2048]{1,0:T(8,128)(2,1)} fusion(bf16[1,512,2048]{2,1,0:T(8,128)(2,1)} %param.29, f32[1024,512]{1,0:T(8,128)} %fusion.2, bf16[1024,2048]{1,0:T(8,128)(2,1)} %bitcast.55, bf16[1,2048,512]{2,1,0:T(8,128)(2,1)} %param.27), kind=kOutput, calls=%fused_computation.1 | convolution fusion | flops 4300210176 | bytes 14680064 | tf_op jit(solution)/shard_map/dot_general | solution.py:577
  122.1 0.0 copy-start.3
  122.1 2.2 %copy-done.3 = bf16[1024,2048]{1,0:T(8,128)(2,1)S(1)} copy-done((bf16[1024,2048]{1,0:T(8,128)(2,1)S(1)}, bf16[1024,2048]{1,0:T(8,128)(2,1)}, u32[]{:S(2)}) %copy-start.3) | copy-done | bytes 4194328
  124.3 46.3 %give_back.1 = bf16[4,64,2048]{2,1,0:T(8,128)(2,1)S(1)} custom-call(bf16[2,4,4,32,2048]{4,3,2,1,0:T(8,128)(2,1)S(1)} %bitcast.52, bf16[4,16,128]{2,1,0:T(8,128)(2,1)S(1)} %get-tuple-element.8.metas_ref), custom_call_target="tpu_custom_call" | custom-call | tf_op jit(solution)/shard_map/give_back/pallas_call | solution.py:360
  170.7 0.0 copy-done.10
  170.7 1.1 fusion
  (24 shorter events, 0.3 us)
Async XLA Ops:
  0.0 43.3 %copy-start = (bf16[768,2048]{1,0:T(8,128)(2,1)S(1)}, bf16[768,2048]{1,0:T(8,128)(2,1)}, u32[]{:S(2)}) copy-start(bf16[768,2048]{1,0:T(8,128)(2,1)} %param.22) | copy-start | bytes 9437188
  7.6 14.1 %copy-start.15 = (s32[256]{0:T(256)S(1)}, s32[256]{0:T(256)}, u32[]{:S(2)}) copy-start(s32[256]{0:T(256)} %param.19) | copy-start | bytes 3076
  20.0 1.6 copy-start.1
  28.8 1.9 %copy-start.2 = (bf16[16,256,384]{2,1,0:T(8,128)(2,1)S(1)}, bf16[16,256,384]{2,1,0:T(8,128)(2,1)}, u32[]{:S(2)}) copy-start(bf16[16,256,384]{2,1,0:T(8,128)(2,1)} %copy-done.1) | copy-start | bytes 9437188
  30.7 0.9 copy-start.4
  31.6 0.9 copy-start.5
  32.5 0.9 copy-start.6
  33.4 0.9 copy-start.7
  34.4 7.6 %copy-start.12 = (s32[128,2]{0,1:T(2,128)S(1)}, s32[128,2]{0,1:T(2,128)}, u32[]{:S(2)}) copy-start(s32[128,2]{0,1:T(2,128)} %param.25) | copy-start | bytes 3076
  34.4 7.7 %copy-start.16 = (f32[128,2]{0,1:T(2,128)S(1)}, f32[128,2]{0,1:T(2,128)}, u32[]{:S(2)}) copy-start(f32[128,2]{0,1:T(2,128)} %param.26) | copy-start | bytes 3076
  38.4 4.9 %all-to-all-start = ((bf16[2,128,384]{1,2,0:T(8,128)(2,1)}), bf16[2,128,384]{1,2,0:T(8,128)(2,1)S(1)}, u32[]{:S(2)}, u32[]{:S(2)}) async-start(bf16[2,128,384]{1,2,0:T(8,128)(2,1)} %copy_bitcast_fusion), calls=%async_computation | async-start | bytes 393216 | tf_op jit(solution)/shard_map/all_to_all | solution.py:524
  43.3 1.0 copy-start.11
  43.3 1.0 copy-start.13
  44.0 0.8 copy-start.14
  44.6 0.8 copy-start.9
  44.6 63.1 %copy-start.17 = (bf16[1,2048,512]{2,1,0:T(8,128)(2,1)S(1)}, bf16[1,2048,512]{2,1,0:T(8,128)(2,1)}, u32[]{:S(2)}) copy-start(bf16[1,2048,512]{2,1,0:T(8,128)(2,1)} %param.28) | copy-start | bytes 6291460
  105.8 1.9 %copy-start.8 = (bf16[2,4,4,32,2048]{4,3,2,1,0:T(8,128)(2,1)}, bf16[2,4,4,32,2048]{4,3,2,1,0:T(8,128)(2,1)S(1)}, u32[]{:S(2)}) copy-start(bf16[2,4,4,32,2048]{4,3,2,1,0:T(8,128)(2,1)S(1)} %get-tuple-element.7) | copy-start | bytes 12582916
  122.1 2.2 %copy-start.3 = (bf16[1024,2048]{1,0:T(8,128)(2,1)S(1)}, bf16[1024,2048]{1,0:T(8,128)(2,1)}, u32[]{:S(2)}) copy-start(bf16[1024,2048]{1,0:T(8,128)(2,1)} %convolution_convert_fusion) | copy-start | bytes 12582916
  124.3 46.3 %copy-start.10 = (bf16[128,2048]{1,0:T(8,128)(2,1)S(1)}, bf16[128,2048]{1,0:T(8,128)(2,1)}, u32[]{:S(2)}) copy-start(bf16[128,2048]{1,0:T(8,128)(2,1)} %copy-done.9) | copy-start | bytes 1572868
